TPU v7x, 256 devices: a whole 4x4x8 slice. The times are simulated.
256 devices in a mesh: sp: 32 (over z, y), tp: 8 (over x, core).
Axes of the slice: x: 4, y: 4, z: 8, core: 2. Of those that a mesh axis runs over, the one named last changes fastest.
Arguments:
- latent: bfloat16 [12288, 2048], P(('sp', 'tp')), may hold values from -6 to 6
- context: bfloat16 [512, 2048], P('sp'), may hold values from -6 to 6
- cond_latent: float32 [2048], replicated, may hold values from -6 to 6
- cond_context: float32 [2048], replicated, may hold values from -12 to 12
- shift_weight: bfloat16 [2048, 2048], P('sp', 'tp'), may hold values from -0.125 to 0.125
- scale_weight: bfloat16 [2048, 2048], P('sp', 'tp'), may hold values from -0.125 to 0.125
- gate_weight: bfloat16 [2048, 2048], P('sp', 'tp'), may hold values from -0.125 to 0.125
- query_weight: bfloat16 [2, 2048, 1024], P(None, None, 'tp'), may hold values from -1.3258252 to 1.3258252
- key_weight: bfloat16 [2, 2048, 1024], P(None, None, 'tp'), may hold values from -1.3258252 to 1.3258252
- value_weight: bfloat16 [2048, 2048], P(None, 'tp'), may hold values from -0.125 to 0.125
- out_weight: bfloat16 [2048, 2048], P('tp'), may hold values from -0.125 to 0.125
- lambda_heads: float32 [16], P('tp'), may hold values from 0.3 to 0.8
- out_gain: float32 [2048], P('tp'), may hold values from 0.1 to 1.9
Outputs:
- result: bfloat16 [12288, 2048], P(('sp', 'tp'))
All inputs are finite; a program needn't handle non-finite values.
Results may differ from a plain program's by a relative error of at most 0.02.
The roundings to bfloat16 on the way count: a program that leaves them out, or rounds other values in their place, can miss the bound.
Values may be sent and summed in bfloat16 or wider, within the bound.
A program may use at most 128 MiB of HBM per device.

v0:
```python
import jax
import jax.numpy as jnp
from jax import lax
from jax.sharding import PartitionSpec as P

HEAD_DIM = 64
GRID_W = 64
VALUE_DIM = 128


norm_eps = 1e-06
rope_theta = 10000.0
block_limit = 1024


def copy_for_each(value, axis):
    copies = jnp.broadcast_to(value, (lax.axis_size(axis), *value.shape))
    return lax.all_to_all(copies, axis, split_axis=0, concat_axis=0, tiled=True)


def taken_together(value, axis):
    return copy_for_each(value, axis).sum(axis=0)


def in_order(tiles, dim):
    dims = list(tiles.shape[1:])
    dims[dim] *= tiles.shape[0]
    return jnp.moveaxis(tiles, 0, dim).reshape(dims)


def gathered_copies(value, axis, dim):
    tiles = copy_for_each(value, axis)
    return in_order(tiles, dim)


def in_one_piece(arrays, axis, dim, along):
    both = jnp.concatenate(arrays, axis=along)
    out, at, gathered = (lax.all_gather(both, axis, axis=dim, tiled=True), 0, [])
    for a in arrays:
        gathered.append(lax.slice_in_dim(out, at, at + a.shape[along], axis=along))
        at += a.shape[along]
    return tuple(gathered)


def in_blocks(value, dim, length):
    before, after = (value.shape[:dim], value.shape[dim + 1 :])
    return jnp.moveaxis(value.reshape(*before, length, -1, *after), dim, 0)


def sent_and_summed(value, axis, dim):
    tiles = in_blocks(value, dim, lax.axis_size(axis))
    arrived = lax.all_to_all(tiles, axis, split_axis=0, concat_axis=0, tiled=True)
    return arrived.astype(jnp.float32).sum(axis=0)


def rms_scale(matrix):
    return matrix * lax.rsqrt(jnp.mean(matrix * matrix, axis=-1, keepdims=True) + norm_eps)


def modulated(activations, shift, scale):
    return (rms_scale(activations.astype(jnp.float32)) * (1.0 + scale) + shift).astype(jnp.bfloat16)


def rotate(vectors, positions, grid_width):
    quarter = vectors.shape[-1] // 4
    inverse = rope_theta ** (-jnp.arange(quarter, dtype=jnp.float32) / quarter)
    grid_row = (positions // grid_width).astype(jnp.float32)
    grid_col = (positions % grid_width).astype(jnp.float32)
    angles = jnp.concatenate([grid_row[:, None] * inverse, grid_col[:, None] * inverse], axis=-1)
    cos_table = jnp.cos(angles)[:, None, :]
    sin_table = jnp.sin(angles)[:, None, :]
    former = vectors[..., : 2 * quarter]
    latter = vectors[..., 2 * quarter :]
    return jnp.concatenate(
        [former * cos_table - latter * sin_table, latter * cos_table + former * sin_table], axis=-1
    )


def absorb(carry_state, key_block, value_block, queries, head_count):
    maxima, totals, numerator = carry_state
    row_count = key_block.shape[0]
    scores = jnp.einsum(
        "mhqd,kmhd->mhqk",
        queries,
        key_block.reshape(row_count, 2, head_count, HEAD_DIM),
        preferred_element_type=jnp.float32,
    ) * HEAD_DIM ** (-0.5)
    new_maxima = jnp.maximum(maxima, jnp.max(scores, axis=-1))
    rescale = jnp.exp(maxima - new_maxima)
    weights = jnp.exp(scores - new_maxima[..., None])
    totals = totals * rescale + jnp.sum(weights, axis=-1)
    numerator = numerator * rescale[..., None] + jnp.einsum(
        "mhqk,khe->mhqe",
        weights.astype(jnp.bfloat16),
        value_block.reshape(row_count, head_count, VALUE_DIM),
        preferred_element_type=jnp.float32,
    )
    return (new_maxima, totals, numerator)


def absorb_all(carry_state, key_rows, value_rows, queries, head_count, shard_len):
    total_rows = key_rows.shape[0]
    shards = total_rows // shard_len
    shard_group = max(
        [
            candidate
            for candidate in range(1, shards + 1)
            if shards % candidate == 0 and candidate * shard_len <= block_limit
        ]
        + [1]
    )
    block_rows = shard_group * shard_len

    def absorb_block(block_index, inner_state):
        key_block = lax.dynamic_slice_in_dim(key_rows, block_index * block_rows, block_rows, 0)
        value_block = lax.dynamic_slice_in_dim(value_rows, block_index * block_rows, block_rows, 0)
        return absorb(inner_state, key_block, value_block, queries, head_count)

    return lax.fori_loop(0, total_rows // block_rows, absorb_block, carry_state)


def local(
    latent,
    context,
    cond_latent,
    cond_context,
    shift_weight,
    scale_weight,
    gate_weight,
    query_weight,
    key_weight,
    value_weight,
    out_weight,
    lambda_heads,
    out_gain,
):
    mod_rows = shift_weight.shape[0]
    conditions = jnp.stack([cond_latent, cond_context])
    conditions = jax.nn.silu(
        lax.dynamic_slice_in_dim(conditions, lax.axis_index("sp") * mod_rows, mod_rows, 1)
    )
    conditions = conditions.astype(jnp.bfloat16)
    partial_value = jnp.concatenate(
        [
            jnp.dot(conditions, shift_weight, preferred_element_type=jnp.float32),
            jnp.dot(conditions, scale_weight, preferred_element_type=jnp.float32),
            jnp.dot(conditions[:1], gate_weight, preferred_element_type=jnp.float32),
        ],
        axis=0,
    )
    summed_mod = taken_together(partial_value, "sp")
    whole_mod = gathered_copies(summed_mod, "tp", 1)
    hidden = modulated(latent, whole_mod[0], whole_mod[2])
    context_hidden = modulated(context, whole_mod[1], whole_mod[3])
    head_count = lambda_heads.shape[0]
    own_rows = latent.shape[0]
    tok_rows = own_rows * lax.axis_size("tp")
    row_offset = lax.axis_index("sp") * tok_rows
    piece_rows = gathered_copies(hidden, "tp", 0)
    row_count = piece_rows.shape[0]
    positions = row_offset + jnp.arange(row_count, dtype=jnp.int32)

    def rotated(weight):
        product = jnp.concatenate(
            [
                jnp.dot(piece_rows, weight[0], preferred_element_type=jnp.float32),
                jnp.dot(piece_rows, weight[1], preferred_element_type=jnp.float32),
            ],
            axis=-1,
        )
        turned = rotate(product.reshape(row_count, 2 * head_count, HEAD_DIM), positions, GRID_W)
        return turned.reshape(row_count, 2 * head_count * HEAD_DIM).astype(jnp.bfloat16)

    values = jnp.dot(piece_rows, value_weight, preferred_element_type=jnp.float32).astype(
        jnp.bfloat16
    )
    projected = jnp.concatenate([rotated(query_weight), rotated(key_weight), values], axis=-1)
    key_width = 2 * head_count * HEAD_DIM
    queries = (
        projected[:, :key_width].reshape(tok_rows, 2, head_count, HEAD_DIM).transpose(1, 2, 0, 3)
    )
    latent_keys = projected[:, key_width : 2 * key_width]
    latent_values = projected[:, 2 * key_width :]
    context_keys = jnp.concatenate(
        [
            jnp.dot(context_hidden, key_weight[0], preferred_element_type=jnp.float32),
            jnp.dot(context_hidden, key_weight[1], preferred_element_type=jnp.float32),
        ],
        axis=-1,
    ).astype(jnp.bfloat16)
    context_values = jnp.dot(
        context_hidden, value_weight, preferred_element_type=jnp.float32
    ).astype(jnp.bfloat16)
    initial = (
        jnp.full((2, head_count, tok_rows), -jnp.inf, jnp.float32),
        jnp.zeros((2, head_count, tok_rows), jnp.float32),
        jnp.zeros((2, head_count, tok_rows, VALUE_DIM), jnp.float32),
    )
    all_context = in_one_piece((context_keys, context_values), "sp", 0, 1)
    started = absorb_all(
        initial, all_context[0], all_context[1], queries, head_count, all_context[0].shape[0]
    )
    pieces = in_one_piece((latent_keys, latent_values), "sp", 0, 1)
    final = absorb_all(started, pieces[0], pieces[1], queries, head_count, tok_rows)
    totals = final[1]
    numerator = final[2]
    mixed = numerator[0] / totals[0][..., None] - lambda_heads[:, None, None] * (
        numerator[1] / totals[1][..., None]
    )
    normed = rms_scale(mixed) * out_gain.reshape(head_count, 1, VALUE_DIM)
    heads_out = (
        normed.transpose(1, 0, 2).reshape(tok_rows, head_count * VALUE_DIM).astype(jnp.bfloat16)
    )
    summed = sent_and_summed(
        jnp.dot(heads_out, out_weight, preferred_element_type=jnp.float32).astype(jnp.bfloat16),
        "tp",
        0,
    )
    return (latent.astype(jnp.float32) + whole_mod[4] * summed).astype(jnp.bfloat16)


def solution(mesh):
    placed = (
        P(("sp", "tp"), None),
        P("sp", None),
        P(),
        P(),
        P("sp", "tp"),
        P("sp", "tp"),
        P("sp", "tp"),
        P(None, None, "tp"),
        P(None, None, "tp"),
        P(None, "tp"),
        P("tp", None),
        P("tp"),
        P("tp"),
    )
    return jax.shard_map(
        local, mesh=mesh, in_specs=placed, out_specs=P(("sp", "tp"), None), check_vma=False
    )
```

profile of v0, /device:TPU:1, one launch (start us, length us, event | category | flops | bytes accessed | tf_op | source)
XLA Modules:
  0.0 302.4 jit_solution(11932503961697550053)
XLA Ops:
  10.8 12.0 %all-to-all-start = ((f32[32,5,256]{2,1,0:T(8,128)}), f32[32,5,256]{2,1,0:T(8,128)S(1)}, u32[]{:S(2)}, u32[]{:S(2)}) async-start(f32[32,5,256]{2,1,0:T(8,128)} %broadcast_in_dim.16), calls=%async_computation | async-start | bytes 524288 | tf_op jit(solution)/shard_map/all_to_all | solution.py:18
  23.9 10.2 %all-to-all-done = f32[32,5,256]{2,1,0:T(8,128)S(1)} async-done(((f32[32,5,256]{2,1,0:T(8,128)}), f32[32,5,256]{2,1,0:T(8,128)S(1)}, u32[]{:S(2)}, u32[]{:S(2)}) %all-to-all-start) | async-done | bytes 163872 | tf_op jit(solution)/shard_map/all_to_all | solution.py:18
  34.8 6.8 %all-to-all-start.1 = ((f32[8,5,256]{2,1,0:T(8,128)}), f32[8,5,256]{2,1,0:T(8,128)S(1)}, u32[]{:S(2)}, u32[]{:S(2)}) async-start(f32[8,5,256]{2,1,0:T(8,128)} %broadcast_in_dim.17), calls=%async_computation.1 | async-start | bytes 131072 | tf_op jit(solution)/shard_map/all_to_all | solution.py:18
  41.5 4.8 %all-to-all-done.1 = f32[8,5,256]{2,1,0:T(8,128)S(1)} async-done(((f32[8,5,256]{2,1,0:T(8,128)}), f32[8,5,256]{2,1,0:T(8,128)S(1)}, u32[]{:S(2)}, u32[]{:S(2)}) %all-to-all-start.1) | async-done | bytes 40992 | tf_op jit(solution)/shard_map/all_to_all | solution.py:18
  47.5 1.3 broadcast_in_dim.18
  48.8 4.3 %all-to-all-start.2 = ((bf16[8,48,2048]{2,1,0:T(8,128)(2,1)}), bf16[8,48,2048]{2,1,0:T(8,128)(2,1)S(1)}, u32[]{:S(2)}, u32[]{:S(2)}) async-start(bf16[8,48,2048]{2,1,0:T(8,128)(2,1)} %broadcast_in_dim.18), calls=%async_computation.2 | async-start | bytes 3145728 | tf_op jit(solution)/shard_map/all_to_all | solution.py:18
  53.4 20.3 %all-to-all-done.2 = bf16[8,48,2048]{2,1,0:T(8,128)(2,1)S(1)} async-done(((bf16[8,48,2048]{2,1,0:T(8,128)(2,1)}), bf16[8,48,2048]{2,1,0:T(8,128)(2,1)S(1)}, u32[]{:S(2)}, u32[]{:S(2)}) %all-to-all-start.2) | async-done | bytes 1572896 | tf_op jit(solution)/shard_map/all_to_all | solution.py:18
  73.7 1.8 fusion.27
  80.2 38.0 %all_gather.6 = bf16[512,512]{1,0:T(8,128)(2,1)S(1)} all-gather(bf16[16,512]{1,0:T(8,128)(2,1)S(1)} %pad_maximum_fusion.6), channel_id=1, replica_groups=mesh['sp'=32,'tp'=8] {'sp'}, dimensions={0}, use_global_device_ids=true | all-gather | bytes 540672 | tf_op jit(solution)/shard_map/all_gather | solution.py:38
  120.8 75.6 %all-gather.2.cloned.1.call-done = bf16[12288,512]{0,1:T(8,128)(2,1)} async-done(((bf16[384,512]{0,1:T(8,128)(2,1)}), bf16[12288,512]{0,1:T(8,128)(2,1)}) %all-gather.2.cloned.1.call-update) | async-done | bytes 12582928 | tf_op jit(solution)/shard_map/all_gather | solution.py:38
  196.4 10.4 %fusion.66 = (bf16[12288,256]{0,1:T(8,128)(2,1)}, bf16[12288,256]{0,1:T(8,128)(2,1)}) fusion(bf16[12288,512]{0,1:T(8,128)(2,1)} %all-gather.2.cloned.1.call-done), kind=kLoop, calls=%fused_computation.110 | loop fusion | bytes 25165824 | tf_op jit(solution)/shard_map/slice | solution.py:40
  206.8 58.1 %while.4 = (s32[]{:T(128)}, f32[2,2,384]{2,1,0:T(2,128)S(1)}, f32[2,2,384]{2,1,0:T(2,128)S(1)}, f32[2,2,384,128]{2,3,0,1:T(8,128)S(1)}, bf16[12288,256]{0,1:T(8,...) while((s32[]{:T(128)}, f32[2,2,384]{2,1,0:T(2,128)S(1)}, ...), condition=%wide.region_8.9_spmd, body=%wide.region_5.8_spmd.sunk | while | flops 460459008 | bytes 18389152 | solution.py:119
  206.9 1.2 constant_dynamic-slice_fusion.3
  210.5 1.2 constant_dynamic-slice_fusion.3
  214.1 1.2 constant_dynamic-slice_fusion.3
  217.8 1.2 constant_dynamic-slice_fusion.3
  221.4 1.2 constant_dynamic-slice_fusion.3
  225.0 1.2 constant_dynamic-slice_fusion.3
  228.6 1.2 constant_dynamic-slice_fusion.3
  232.3 1.2 constant_dynamic-slice_fusion.3
  235.9 1.2 constant_dynamic-slice_fusion.3
  243.2 1.2 constant_dynamic-slice_fusion.3
  254.0 1.2 constant_dynamic-slice_fusion.3
  265.9 28.7 %all_to_all.20 = bf16[8,48,2048]{2,1,0:T(8,128)(2,1)S(1)} all-to-all(bf16[8,48,2048]{2,1,0:T(8,128)(2,1)S(1)} %bitcast.133), channel_id=1, replica_groups=mesh['sp'=32,'tp'=8] {'tp'}, dimensions={0} | all-to-all | bytes 3145728 | tf_op jit(solution)/shard_map/all_to_all | solution.py:52
  (186 shorter events, 60.5 us)
Async XLA Ops:
  6.5 258.7 %copy-start = (bf16[256,2048]{1,0:T(8,128)(2,1)S(1)}, bf16[256,2048]{1,0:T(8,128)(2,1)}, u32[]{:S(2)}) copy-start(bf16[256,2048]{1,0:T(8,128)(2,1)} %param.25) | copy-start | bytes 3145732
  10.8 23.3 %all-to-all-start = ((f32[32,5,256]{2,1,0:T(8,128)}), f32[32,5,256]{2,1,0:T(8,128)S(1)}, u32[]{:S(2)}, u32[]{:S(2)}) async-start(f32[32,5,256]{2,1,0:T(8,128)} %broadcast_in_dim.16), calls=%async_computation | async-start | bytes 524288 | tf_op jit(solution)/shard_map/all_to_all | solution.py:18
  34.8 11.6 %all-to-all-start.1 = ((f32[8,5,256]{2,1,0:T(8,128)}), f32[8,5,256]{2,1,0:T(8,128)S(1)}, u32[]{:S(2)}, u32[]{:S(2)}) async-start(f32[8,5,256]{2,1,0:T(8,128)} %broadcast_in_dim.17), calls=%async_computation.1 | async-start | bytes 131072 | tf_op jit(solution)/shard_map/all_to_all | solution.py:18
  48.8 24.9 %all-to-all-start.2 = ((bf16[8,48,2048]{2,1,0:T(8,128)(2,1)}), bf16[8,48,2048]{2,1,0:T(8,128)(2,1)S(1)}, u32[]{:S(2)}, u32[]{:S(2)}) async-start(bf16[8,48,2048]{2,1,0:T(8,128)(2,1)} %broadcast_in_dim.18), calls=%async_computation.2 | async-start | bytes 3145728 | tf_op jit(solution)/shard_map/all_to_all | solution.py:18
  53.1 143.3 %all-gather.2.cloned.1.call-start = ((), (), s32[]{:S(2)}) async-start(), calls=%async_computation.4 | async-start | bytes 12976128 | tf_op jit(solution)/shard_map/all_gather | solution.py:38
  73.7 1.8 copy-start.4
  73.7 2.4 copy-start.5
  76.1 1.2 copy-start.1
  78.1 1.1 copy-start.7
  78.1 1.3 copy-start.6
  78.1 1.8 copy-start.2
  206.8 58.1 %copy-start.9 = (f32[2]{0:T(128)S(1)}, f32[2]{0:T(128)}, u32[]{:S(2)}) copy-start(f32[2]{0:T(128)} %param.26) | copy-start | bytes 28
  206.8 58.3 %copy-start.8 = (f32[256]{0:T(256)S(1)}, f32[256]{0:T(256)}, u32[]{:S(2)}) copy-start(f32[256]{0:T(256)} %param.27) | copy-start | bytes 3076
  265.8 29.0 %copy-start.3 = (bf16[48,2048]{1,0:T(8,128)(2,1)S(1)}, bf16[48,2048]{1,0:T(8,128)(2,1)}, u32[]{:S(2)}) copy-start(bf16[48,2048]{1,0:T(8,128)(2,1)} %param.15) | copy-start | bytes 589828
Sparse Core Ops, SparseCore 0:
  79.3 117.0 all-gather.1
where the time goes:
time: 303 us; the launch traced here: 302 us
  waiting for transfers between devices  111 us (37%)
  blocking collectives  66.7 us (22%)
  matrix products  33 us (11%)
  local copies, waits for them, and re-layouts  32.5 us (11%)
  starting transfers between devices  23 us (8%)
  other arithmetic  21.4 us (7%)
  between operations  13.7 us (5%)
    all_gather x1, waiting for transfers between devices, in_one_piece(): lax.all_gather(both, axis, axis=dim, tiled=True)  75.6 us
    all_gather x1, blocking collectives, in_one_piece(): lax.all_gather(both, axis, axis=dim, tiled=True)  38 us
    all_to_all x3, waiting for transfers between devices, copy_for_each(): return lax.all_to_all(copies, axis, split_axis=0, concat_axis=0, tiled=True)  35.4 us
    all_to_all x1, blocking collectives, sent_and_summed(): lax.all_to_all(tiles, axis, split_axis=0, concat_axis=0, tiled=True)  28.7 us
    all_to_all x3, starting transfers between devices, copy_for_each(): return lax.all_to_all(copies, axis, split_axis=0, concat_axis=0, tiled=True)  23 us
    dynamic_slice x16, local copies, waits for them, and re-layouts, absorb_block(): lax.dynamic_slice_in_dim(value_rows, block_index * block_rows, block_rows...  18.8 us
    convert_element_type x17, other arithmetic, absorb(): weights.astype(jnp.bfloat16)  15.2 us
    dot_general x17, matrix products, absorb(): jnp.einsum('mhqd,kmhd->mhqk', queries, key_block.reshape(row_count, 2, he...  14.2 us
  transfers between devices with their start and end apart: 4, of which 4 were waited for; matrix products, arithmetic and copies ran while one was open for 2% of the time, Pallas kernels for 0%

commit v1 on v0

v1 whole, which is shorter than its diff:
```python
import functools

import jax
import jax.numpy as jnp
from jax import lax
from jax.experimental import pallas as pl
from jax.experimental.pallas import tpu as pltpu
from jax.sharding import PartitionSpec as P

HEAD_DIM = 64
GRID_W = 64
VALUE_DIM = 128
NX, NY, NZ, NC = 4, 4, 8, 2

norm_eps = 1e-06
rope_theta = 10000.0
log2_e = 1.4426950408889634

MESH = pl.DeviceIdType.MESH
F32, BF16 = jnp.float32, jnp.bfloat16
NT = (((1,), (1,)), ((), ()))


def send(src, dst, send_sem, recv_sem, device):
    pltpu.make_async_remote_copy(
        src_ref=src, dst_ref=dst, send_sem=send_sem, recv_sem=recv_sem,
        device_id=device, device_id_type=MESH,
    ).start()


def landed(ref, sem):
    pltpu.make_async_copy(ref, ref, sem).wait()


class Around:
    def __init__(self, buf, first, second, sems, x, c, place):
        self.buf, self.first, self.second, self.place = buf, first, second, place
        self.send, self.recv, self.dsend, self.drecv = sems
        self.c = c
        self.x = x
        self.xl, self.xr, self.xa = (x + 3) % NX, (x + 1) % NX, (x + 2) % NX

    def at(self, x, c=None):
        return self.buf.at[x * NC + (self.c if c is None else c)]

    def start(self, src):
        own, other = self.at(self.x), self.place(self.x, 1 - self.c)
        send(src, own, self.send.at[0], self.recv.at[0], self.place(self.xr, self.c))
        send(src, own, self.send.at[1], self.recv.at[1], self.place(self.xl, self.c))
        send(src, own, self.dsend.at[0], self.drecv.at[0], other)

    def forward(self):
        left, right, other = self.at(self.xl), self.at(self.xr), self.place(self.x, 1 - self.c)
        landed(left, self.recv.at[0])
        a = self.first(left)
        send(a, a, self.send.at[2], self.recv.at[2], self.place(self.xr, self.c))
        landed(right, self.recv.at[1])
        b = self.second(right)
        send(b, b, self.send.at[3], self.recv.at[3], self.place(self.xl, self.c))
        send(left, left, self.dsend.at[1], self.drecv.at[1], other)
        send(right, right, self.dsend.at[2], self.drecv.at[2], other)

    def last(self):
        far, other = self.at(self.xa), self.place(self.x, 1 - self.c)
        landed(self.first(far), self.recv.at[2])
        landed(self.second(far), self.recv.at[3])
        send(far, far, self.dsend.at[3], self.drecv.at[3], other)

    def finish(self):
        for k, at in enumerate((self.x, self.xl, self.xr, self.xa)):
            landed(self.at(at, 1 - self.c), self.drecv.at[k])

    def drain(self, src):
        landed(src, self.send.at[0])
        landed(src, self.send.at[1])
        landed(src, self.dsend.at[0])
        landed(self.first(self.at(self.xl)), self.send.at[2])
        landed(self.second(self.at(self.xr)), self.send.at[3])
        for k, at in enumerate((self.xl, self.xr, self.xa)):
            landed(self.at(at), self.dsend.at[k + 1])


def attend(qs, m, acc, k, v, sbuf, block):
    n = qs.shape[0] // block
    width = k.shape[0]
    v1 = jnp.concatenate([v, jnp.ones(v.shape, v.dtype)], axis=1)

    def scores(i):
        return lax.dot_general(qs[pl.ds(i * block, block), :], k, NT, preferred_element_type=F32)

    sbuf[0, :, :width] = scores(0)
    for i in range(n):
        if i + 1 < n:
            sbuf[(i + 1) % 2, :, :width] = scores(i + 1)
        rows = pl.ds(i * block, block)
        s = sbuf[i % 2, :, :width]
        before = m[rows, :]
        after = jnp.maximum(before, jnp.max(s, axis=1, keepdims=True))
        p = jnp.exp2(s - after[:, :1]).astype(BF16)
        rescale = jnp.exp2(before - after)
        m[rows, :] = after
        pv = jnp.dot(p, v1, preferred_element_type=F32)
        acc[rows, :] = acc[rows, :] * jnp.concatenate([rescale, rescale], axis=1) + pv


def kernel(
    tok, ctxr,
    lat, ctx, lhs, shw, scw, gaw, extra, cos, sin, wq, wk, wv, wo, out,
    zbuf, ybuf, tbuf, modw, lbuf, hid, w, wall, qst, kst, vst, qbuf, kv, qs, m, acc, sbuf, obuf, hb,
    wsem, zs_s, zs_r, ys_s, ys_r, ts_s, ts_r,
    l_s, l_r, l_ds, l_dr, w_s, w_r, w_ds, w_dr,
    q_s, q_r, k_s, v_s, kv_r, own_s, fwd_s, ring_r, d_s, d_r, o_s, o_r,
):
    sp, tp = lax.axis_index("sp"), lax.axis_index("tp")
    z, y = sp // NY, sp % NY
    x, c = tp // NC, tp % NC

    def place(px, pc, py=None, pz=None):
        return ((z if pz is None else pz) * NY + (y if py is None else py), px * NC + pc)

    loads = [
        pltpu.make_async_copy(wo, wall.at[tp], wsem.at[0]),
        pltpu.make_async_copy(wq.at[0], w.at[:, pl.ds(0, 128)], wsem.at[1]),
        pltpu.make_async_copy(wq.at[1], w.at[:, pl.ds(128, 128)], wsem.at[2]),
        pltpu.make_async_copy(wk.at[0], w.at[:, pl.ds(256, 128)], wsem.at[3]),
        pltpu.make_async_copy(wk.at[1], w.at[:, pl.ds(384, 128)], wsem.at[4]),
        pltpu.make_async_copy(wv, w.at[:, pl.ds(512, 256)], wsem.at[5]),
    ]
    for load in loads:
        load.start()

    barrier = pltpu.get_barrier_semaphore()
    others = [(dx, dy, dc) for dx in range(NX) for dy in range(NY) for dc in range(NC)][1:]
    for dz in range(1, NZ):
        pl.semaphore_signal(barrier, inc=1, device_id=place(x, c, pz=(z + dz) % NZ), device_id_type=MESH)
    for dx, dy, dc in others:
        pl.semaphore_signal(
            barrier, inc=1, device_id=place((x + dx) % NX, (c + dc) % NC, py=(y + dy) % NY), device_id_type=MESH
        )

    part = jnp.dot(lhs[0], shw[...], preferred_element_type=F32)
    part += jnp.dot(lhs[1], scw[...], preferred_element_type=F32)
    part += jnp.dot(lhs[2], gaw[...], preferred_element_type=F32)
    zbuf[z] = part[:8]
    lbuf[tp] = lat[...]

    pl.semaphore_wait(barrier, NZ - 1 + len(others))

    for d in range(1, NZ):
        send(zbuf.at[z], zbuf.at[z], zs_s.at[d - 1], zs_r.at[d - 1], place(x, c, pz=(z + d) % NZ))
    rows = Around(
        lbuf, lambda r: r.at[:, pl.ds(0, 1024)], lambda r: r.at[:, pl.ds(1024, 1024)], (l_s, l_r, l_ds, l_dr), x, c, place
    )
    rows.start(lat)
    for d in range(1, NZ):
        landed(zbuf.at[(z - d + NZ) % NZ], zs_r.at[d - 1])
    total = zbuf[0]
    for k in range(1, NZ):
        total += zbuf[k]
    ybuf[y] = total
    for d in range(1, NY):
        send(ybuf.at[y], ybuf.at[y], ys_s.at[d - 1], ys_r.at[d - 1], place(x, c, py=(y + d) % NY))
    for d in range(1, NY):
        landed(ybuf.at[(y - d + NY) % NY], ys_r.at[d - 1])
    tbuf[tp] = (ybuf[0] + ybuf[1]) + (ybuf[2] + ybuf[3]) + extra[...]
    tps = [(dx, dc) for dx in range(NX) for dc in range(NC)][1:]
    for k, (dx, dc) in enumerate(tps):
        send(tbuf.at[tp], tbuf.at[tp], ts_s.at[k], ts_r.at[k], place((x + dx) % NX, (c + dc) % NC))
    rows.forward()
    for k, (dx, dc) in enumerate(tps):
        landed(tbuf.at[((x - dx + NX) % NX) * NC + (c + dc) % NC], ts_r.at[k])
    for k in range(NX * NC):
        modw[:, k * 256 : (k + 1) * 256] = tbuf[k]
    rows.last()

    loads[0].wait()
    weights = Around(
        wall, lambda r: r.at[pl.ds(0, 128)], lambda r: r.at[pl.ds(128, 128)], (w_s, w_r, w_ds, w_dr), x, c, place
    )
    weights.start(wall.at[tp])
    rows.finish()

    def modulate(values, shift, scale):
        values = values.astype(F32)
        inverse = lax.rsqrt(jnp.mean(values * values, axis=-1, keepdims=True) + norm_eps)
        return (values * inverse * (1.0 + scale) + shift).astype(BF16)

    own_rows = lat.shape[0]

    def one_block(k, _):
        hid[pl.ds(pl.multiple_of(k * own_rows, 16), own_rows), :] = modulate(lbuf[k], modw[0:1, :], modw[2:3, :])
        return 0

    lax.fori_loop(0, NX * NC, one_block, 0)
    hid[tok : tok + ctxr, :] = modulate(ctx[...], modw[1:2, :], modw[3:4, :])
    for load in loads[1:]:
        load.wait()

    lane = lax.broadcasted_iota(jnp.int32, (tok + ctxr, 128), 1)
    low_half, low_head = lane % 64 < 32, lane < 64

    def turned(u):
        swapped = jnp.where(low_half, pltpu.roll(u, 96, 1), pltpu.roll(u, 32, 1))
        return u * cos[...] + swapped * sin[...]

    def by_head(both):
        m1, m2 = turned(both[:, :128]), turned(both[:, 128:])
        return (
            jnp.where(low_head, m1, pltpu.roll(m2, 64, 1)),
            jnp.where(low_head, pltpu.roll(m1, 64, 1), m2),
        )

    keys = by_head(jnp.dot(hid[...], w[:, 256:512], preferred_element_type=F32))
    kst[0], kst[1] = keys[0].astype(BF16), keys[1].astype(BF16)
    vals = jnp.dot(hid[...], w[:, 512:768], preferred_element_type=F32).astype(BF16)
    vst[0], vst[1] = vals[:, :128], vals[:, 128:]

    def self_head(j):
        return 2 * c + j == y

    for j in range(2):
        yd = 2 * c + j
        off = (y - yd + NY) % NY

        @pl.when(jnp.logical_or(yd != y, c != 0))
        def _():
            send(kst.at[j], kv.at[0, z, off], k_s.at[j], kv_r.at[off], place(x, 0, py=yd))

        @pl.when(jnp.logical_and(yd == y, c == 0))
        def _():
            kv[0, z, 0] = kst[j]

        @pl.when(jnp.logical_or(yd != y, c != 1))
        def _():
            send(vst.at[j], kv.at[1, z, off], v_s.at[j], kv_r.at[off], place(x, 1, py=yd))

        @pl.when(jnp.logical_and(yd == y, c == 1))
        def _():
            kv[1, z, 0] = vst[j]

    heads = by_head(jnp.dot(hid[...], w[:, 0:256], preferred_element_type=F32))
    for j in range(2):
        qst[j] = (heads[j][:tok] * (log2_e * HEAD_DIM**-0.5)).astype(BF16)
    for j in range(2):
        yd = 2 * c + j

        @pl.when(yd != y)
        def _():
            send(qst.at[j], qbuf.at[y % 2], q_s.at[j], q_r.at[y % 2], place(x, y // 2, py=yd))

        @pl.when(yd == y)
        def _():
            qbuf[y % 2] = qst[j]

    m[...] = jnp.full(m.shape, -jnp.inf, F32)
    acc[...] = jnp.zeros(acc.shape, F32)

    up, down, other = place(x, c, pz=(z + 1) % NZ), place(x, c, pz=(z + NZ - 1) % NZ), place(x, 1 - c)

    def half(zs, p):
        return kv.at[c, zs, pl.ds(2 * p, 2)]

    for p in range(2):
        if p == 0:

            @pl.when(c != y // 2)
            def _():
                landed(kv.at[c, z, 0], kv_r.at[0])
        else:
            landed(kv.at[c, z, 2], kv_r.at[2])
        landed(kv.at[c, z, 2 * p + 1], kv_r.at[2 * p + 1])
        mine = half(z, p)
        send(mine, mine, own_s.at[0, p], ring_r.at[1, p], up)
        send(mine, mine, own_s.at[1, p], ring_r.at[2, p], down)
        send(mine, mine, d_s.at[0, p], d_r.at[0, p], other)

    for i in range(2):

        @pl.when(2 * c + i != y)
        def _():
            landed(qbuf.at[i], q_r.at[i])

    low = lax.broadcasted_iota(jnp.int32, (tok, 128), 1) < 64
    for i in range(2):
        q = qbuf[i]
        nothing = jnp.zeros_like(q)
        qs[i * tok : (i + 1) * tok, :] = jnp.where(low, q, nothing)
        qs[(2 + i) * tok : (3 + i) * tok, :] = jnp.where(low, nothing, q)

    def source(u):
        return (z + (2 * ((u + 1) % 2) - 1) * ((u + 1) // 2) + NZ) % NZ

    def chunk(u, _):
        @pl.when(u == 4)
        def _():
            weights.forward()

        @pl.when(u == 6)
        def _():
            weights.last()

        zs = source(u)
        for p in range(2):
            piece = half(zs, p)

            @pl.when(u >= 1)
            def _():
                landed(piece, ring_r.at[u, p])
                if p == 0:
                    goes, later = u <= 5, u + 2
                else:
                    goes, later = jnp.logical_or(u <= 4, u == 6), u + 2 - u // 6
                side = (u + 1) % 2
                nz = (z + 1 - 2 * side + NZ) % NZ

                @pl.when(goes)
                def _():
                    send(piece, piece, fwd_s.at[u, p], ring_r.at[later, p], place(x, c, pz=nz))

                send(piece, piece, d_s.at[u, p], d_r.at[u, p], other)

        for p in range(2):
            landed(kv.at[1 - c, zs, pl.ds(2 * p, 2)], d_r.at[u, p])
        k = kv[0, zs, :, 0:tok, :].reshape(NY * tok, 128)
        v = kv[1, zs, :, 0:tok, :].reshape(NY * tok, 128)
        attend(qs, m, acc, k, v, sbuf, sbuf.shape[1])
        return 0

    lax.fori_loop(0, NZ, chunk, 0)
    k = kv[0, :, :, tok:, :].reshape(NZ * NY * ctxr, 128)
    v = kv[1, :, :, tok:, :].reshape(NZ * NY * ctxr, 128)
    attend(qs, m, acc, k, v, sbuf, sbuf.shape[1])

    both = 2 * tok
    mine = tbuf[2 * x + y // 2]
    picked = jnp.where(y % 2 == 0, mine[:, :128], mine[:, 128:])
    gain, factor = picked[5:6, :], picked[6:7, :]
    mixed = acc[:both, :128] / acc[:both, 128:] - factor * (acc[both:, :128] / acc[both:, 128:])
    normed = mixed * lax.rsqrt(jnp.mean(mixed * mixed, axis=-1, keepdims=True) + norm_eps) * gain
    obuf[...] = normed.astype(BF16).reshape(obuf.shape)
    head = 4 * x + y
    for i in range(2):
        for t in range(NX * NC):
            home = jnp.logical_and(2 * c + i == y, tp == t)

            @pl.when(jnp.logical_not(home))
            def _():
                send(
                    obuf.at[i, t], hb.at[head], o_s.at[i, t], o_r.at[head], (z * NY + 2 * c + i, t)
                )

            @pl.when(home)
            def _():
                hb[head] = obuf[i, t]

    weights.finish()
    for h in range(NX * NY):
        hx, hy = h // NY, h % NY

        @pl.when(jnp.logical_not(jnp.logical_and(jnp.logical_and(hx == x, hy == y), y // 2 == c)))
        def _():
            landed(hb.at[h], o_r.at[h])

    mixed_sum = jnp.zeros((own_rows, wall.shape[2]), F32)
    for g in range(NX * NC):
        pair = jnp.concatenate([hb[2 * g], hb[2 * g + 1]], axis=1)
        mixed_sum += jnp.dot(pair, wall[g], preferred_element_type=F32).astype(BF16).astype(F32)
    out[...] = (lat[...].astype(F32) + modw[4:5, :] * mixed_sum).astype(BF16)

    for d in range(1, NZ):
        landed(zbuf.at[z], zs_s.at[d - 1])
    for d in range(1, NY):
        landed(ybuf.at[y], ys_s.at[d - 1])
    for k in range(len(tps)):
        landed(tbuf.at[tp], ts_s.at[k])
    rows.drain(lat)
    weights.drain(wall.at[tp])
    for j in range(2):
        yd = 2 * c + j

        @pl.when(yd != y)
        def _():
            landed(qst.at[j], q_s.at[j])

        @pl.when(jnp.logical_or(yd != y, c != 0))
        def _():
            landed(kst.at[j], k_s.at[j])

        @pl.when(jnp.logical_or(yd != y, c != 1))
        def _():
            landed(vst.at[j], v_s.at[j])

    for p in range(2):
        for side in range(2):
            landed(half(z, p), own_s.at[side, p])
        for u in range(NZ):
            landed(half(z, p), d_s.at[u, p])
            if u >= 1 and (u <= 5 if p == 0 else u <= 4 or u == 6):
                landed(half(z, p), fwd_s.at[u, p])
    for i in range(2):
        for t in range(NX * NC):

            @pl.when(jnp.logical_not(jnp.logical_and(2 * c + i == y, tp == t)))
            def _():
                landed(obuf.at[i, t], o_s.at[i, t])


def tables(sp, tok, ctxr):
    quarter = HEAD_DIM // 4
    inverse = rope_theta ** (-jnp.arange(quarter, dtype=F32) / quarter)
    positions = sp * tok + jnp.arange(tok, dtype=jnp.int32)
    grid_row = (positions // GRID_W).astype(F32)
    grid_col = (positions % GRID_W).astype(F32)
    angles = jnp.concatenate([grid_row[:, None] * inverse, grid_col[:, None] * inverse], axis=-1)
    cos, sin = jnp.cos(angles), jnp.sin(angles)
    cos = jnp.concatenate([cos, cos, cos, cos], axis=-1)
    sin = jnp.concatenate([-sin, sin, -sin, sin], axis=-1)
    return (
        jnp.concatenate([cos, jnp.ones((ctxr, 128), F32)], axis=0),
        jnp.concatenate([sin, jnp.zeros((ctxr, 128), F32)], axis=0),
    )


def local(
    latent, context, cond_latent, cond_context, shift_weight, scale_weight, gate_weight,
    query_weight, key_weight, value_weight, out_weight, lambda_heads, out_gain,
):
    own_rows, width = latent.shape
    ctxr = context.shape[0]
    tok = own_rows * NX * NC
    sp = lax.axis_index("sp")
    mod_rows = shift_weight.shape[0]
    conditions = jnp.stack([cond_latent, cond_context])
    conditions = jax.nn.silu(lax.dynamic_slice_in_dim(conditions, sp * mod_rows, mod_rows, 1)).astype(BF16)
    lhs = jnp.stack(
        [
            jnp.pad(conditions, ((0, 14), (0, 0))),
            jnp.pad(conditions, ((2, 12), (0, 0))),
            jnp.pad(conditions[:1], ((4, 11), (0, 0))),
        ]
    )
    extra = jnp.concatenate(
        [
            jnp.zeros((5, 256), F32),
            out_gain[None],
            jnp.repeat(lambda_heads, VALUE_DIM)[None],
            jnp.zeros((1, 256), F32),
        ],
        axis=0,
    )
    cos, sin = tables(sp, tok, ctxr)
    vmem = pl.BlockSpec(memory_space=pltpu.VMEM)
    hbm = pl.BlockSpec(memory_space=pl.ANY)
    dma = pltpu.SemaphoreType.DMA
    block = 256
    return pl.pallas_call(
        functools.partial(kernel, tok, ctxr),
        out_shape=jax.ShapeDtypeStruct((own_rows, width), BF16),
        in_specs=[vmem] * 9 + [hbm] * 4,
        out_specs=vmem,
        scratch_shapes=[
            pltpu.VMEM((NZ, 8, 256), F32),
            pltpu.VMEM((NY, 8, 256), F32),
            pltpu.VMEM((NX * NC, 8, 256), F32),
            pltpu.VMEM((8, width), F32),
            pltpu.VMEM((NX * NC, own_rows, width), BF16),
            pltpu.VMEM((tok + ctxr, width), BF16),
            pltpu.VMEM((width, 768), BF16),
            pltpu.VMEM((NX * NC, 256, width), BF16),
            pltpu.VMEM((2, tok, 128), BF16),
            pltpu.VMEM((2, tok + ctxr, 128), BF16),
            pltpu.VMEM((2, tok + ctxr, 128), BF16),
            pltpu.VMEM((2, tok, 128), BF16),
            pltpu.VMEM((2, NZ, NY, tok + ctxr, 128), BF16),
            pltpu.VMEM((4 * tok, 128), BF16),
            pltpu.VMEM((4 * tok, 128), F32),
            pltpu.VMEM((4 * tok, 256), F32),
            pltpu.VMEM((2, block, NY * tok), F32),
            pltpu.VMEM((2, NX * NC, own_rows, 128), BF16),
            pltpu.VMEM((NX * NY, own_rows, 128), BF16),
            dma((6,)),
            dma((NZ - 1,)), dma((NZ - 1,)), dma((NY - 1,)), dma((NY - 1,)), dma((7,)), dma((7,)),
            dma((4,)), dma((4,)), dma((4,)), dma((4,)),
            dma((4,)), dma((4,)), dma((4,)), dma((4,)),
            dma((2,)), dma((2,)), dma((2,)), dma((2,)), dma((4,)),
            dma((2, 2)), dma((NZ, 2)), dma((NZ, 2)), dma((NZ, 2)), dma((NZ, 2)),
            dma((2, NX * NC)), dma((NX * NY,)),
        ],
        compiler_params=pltpu.CompilerParams(
            collective_id=0, has_side_effects=True, vmem_limit_bytes=60 * 2**20
        ),
    )(
        latent, context, lhs, shift_weight, scale_weight, gate_weight, extra, cos, sin,
        query_weight, key_weight, value_weight, out_weight,
    )


def solution(mesh):
    placed = (
        P(("sp", "tp"), None), P("sp", None), P(), P(),
        P("sp", "tp"), P("sp", "tp"), P("sp", "tp"),
        P(None, None, "tp"), P(None, None, "tp"), P(None, "tp"), P("tp", None), P("tp"), P("tp"),
    )
    return jax.shard_map(
        local, mesh=mesh, in_specs=placed, out_specs=P(("sp", "tp"), None), check_vma=False
    )
```

time: 303 us -> 101 us (0.33)
  waiting for transfers between devices: 111 us -> 0 us
  Pallas kernels: 0 us -> 93.5 us
  blocking collectives: 66.7 us -> 0 us
  matrix products: 33 us -> 0 us
  local copies, waits for them, and re-layouts: 32.5 us -> 3.42 us
  starting transfers between devices: 23 us -> 0 us
  other arithmetic: 21.4 us -> 3.43 us
  between operations: 13.7 us -> 0.07 us
    pallas_call x0 -> x1, Pallas kernels: none -> 93.5 us  [local(): pl.pallas_call(functools.partial(kernel, tok, ctxr), out_shape=jax.ShapeD...]
    all_gather x1 -> x0, waiting for transfers between devices: 75.6 us -> none  [in_one_piece(): lax.all_gather(both, axis, axis=dim, tiled=True)]
    all_gather x1 -> x0, blocking collectives: 38 us -> none  [in_one_piece(): lax.all_gather(both, axis, axis=dim, tiled=True)]
    all_to_all x3 -> x0, waiting for transfers between devices: 35.4 us -> none  [copy_for_each(): return lax.all_to_all(copies, axis, split_axis=0, concat_axis=0, tiled=True)]
    dot_general x46 -> x0, matrix products: 33 us -> none  [the longest x17 14.2 us: absorb(): jnp.einsum('mhqd,kmhd->mhqk', queries, key_block.reshape(row_count, 2, he...]
    all_to_all x1 -> x0, blocking collectives: 28.7 us -> none  [sent_and_summed(): lax.all_to_all(tiles, axis, split_axis=0, concat_axis=0, tiled=True)]
    all_to_all x3 -> x0, starting transfers between devices: 23 us -> none  [copy_for_each(): return lax.all_to_all(copies, axis, split_axis=0, concat_axis=0, tiled=True)]
    dynamic_slice x16 -> x0, local copies, waits for them, and re-layouts: 18.8 us -> none  [absorb_block(): lax.dynamic_slice_in_dim(value_rows, block_index * block_rows, block_rows...]
  transfers between devices with their start and end apart: 4 -> 0, of which waited for: 4 -> 0; matrix products, arithmetic and copies ran while one was open for 2% -> 0% of each run, Pallas kernels for 0% -> 0%
where the time goes in v1:
time: 101 us; the launch traced here: 100 us
  Pallas kernels  93.5 us (93%)
  other arithmetic  3.43 us (3%)
  local copies, waits for them, and re-layouts  3.42 us (3%)
    pallas_call x1, Pallas kernels, local(): pl.pallas_call(functools.partial(kernel, tok, ctxr), out_shape=jax.ShapeD...  93.5 us
    unnamed x9, local copies, waits for them, and re-layouts  3.01 us

profile of v1, /device:TPU:1, one launch (start us, length us, event | category | flops | bytes accessed | tf_op | source)
XLA Modules:
  0.0 100.4 jit_solution(3497516269486289820)
XLA Ops:
  0.0 0.0 copy-start.1
  0.0 0.0 copy-start
  0.0 0.7 copy-done.1
  0.7 0.0 copy-done
  0.7 0.1 fusion.8
  0.8 0.6 pad_maximum_fusion.1.lhs
  1.5 0.1 broadcast_multiply_fusion.1
  1.5 0.2 fusion
  1.7 0.1 copy.20
  1.9 0.9 select_maximum_fusion.sin
  2.8 0.1 copy.16
  2.9 0.0 copy-start.3
  2.9 0.9 select_maximum_fusion.3.cos
  3.8 0.0 copy-done.3
  3.8 0.1 broadcast_in_dim.20
  3.9 0.1 pad.30.clone
  4.0 0.0 copy-start.2
  4.0 0.7 copy-done.2
  4.6 0.7 maximum_maximum_fusion.extra
  5.3 93.5 %shard_map.127 = bf16[48,2048]{1,0:T(8,128)(2,1)} custom-call(bf16[48,2048]{1,0:T(8,128)(2,1)} %lat.1, bf16[16,2048]{1,0:T(8,128)(2,1)} %ctx.1, bf16[3,16,64]{2,1,0:T(8,128)(2,1)} %pad_maximum_fusion.1.lhs, bf16[64,256]{1,0:T(8,128)(2,1)} %shw.1, bf16[64,256]{1,0:T(8,128)(2,1)} %scw.1, bf16[64,256]{1,0:T(8,128)(2,1)} %gaw.1, ...), custom_call_target="tpu_custom_call" | custom-call | tf_op jit(solution)/shard_map/pallas_call | solution.py:456
  98.8 1.6 %copy.24 = bf16[48,2048]{1,0:T(8,128)(2,1)} copy(bf16[48,2048]{1,0:T(8,128)(2,1)} %shard_map.127) | data formatting | bytes 393216
  (6 shorter events, 0.1 us)
Async XLA Ops:
  0.0 0.7 copy-start.1
  0.0 0.7 copy-start
  2.9 0.9 copy-start.3
  4.0 0.7 copy-start.2

commit v2 on v1

v2 whole, which is shorter than its diff:
```python
import functools

import jax
import jax.numpy as jnp
import numpy as np
from jax import lax
from jax.experimental import pallas as pl
from jax.experimental.pallas import tpu as pltpu
from jax.sharding import PartitionSpec as P

HEAD_DIM = 64
GRID_W = 64
VALUE_DIM = 128
NX, NY, NZ, NC = 4, 4, 8, 2

norm_eps = 1e-06
rope_theta = 10000.0
log2_e = 1.4426950408889634

MESH = pl.DeviceIdType.MESH
F32, BF16 = jnp.float32, jnp.bfloat16
NT = (((1,), (1,)), ((), ()))


def send(src, dst, send_sem, recv_sem, device):
    pltpu.make_async_remote_copy(
        src_ref=src, dst_ref=dst, send_sem=send_sem, recv_sem=recv_sem,
        device_id=device, device_id_type=MESH,
    ).start()


def landed(ref, sem):
    pltpu.make_async_copy(ref, ref, sem).wait()


class Around:
    def __init__(self, buf, first, second, sems, x, c, place, split=False):
        self.split = split
        self.buf, self.first, self.second, self.place = buf, first, second, place
        self.send, self.recv, self.dsend, self.drecv = sems
        self.c = c
        self.x = x
        self.xl, self.xr, self.xa = (x + 3) % NX, (x + 1) % NX, (x + 2) % NX

    def at(self, x, c=None):
        return self.buf.at[x * NC + (self.c if c is None else c)]

    def start(self, src):
        own, other = self.at(self.x), self.place(self.x, 1 - self.c)
        send(src, own, self.send.at[0], self.recv.at[0], self.place(self.xr, self.c))
        send(src, own, self.send.at[1], self.recv.at[1], self.place(self.xl, self.c))
        send(src, own, self.dsend.at[0], self.drecv.at[0], other)

    def forward(self):
        left, right, other = self.at(self.xl), self.at(self.xr), self.place(self.x, 1 - self.c)
        landed(left, self.recv.at[0])
        a = self.first(left)
        send(a, a, self.send.at[2], self.recv.at[2], self.place(self.xr, self.c))
        landed(right, self.recv.at[1])
        b = self.second(right)
        send(b, b, self.send.at[3], self.recv.at[3], self.place(self.xl, self.c))
        if not self.split:
            send(left, left, self.dsend.at[1], self.drecv.at[1], other)
            send(right, right, self.dsend.at[2], self.drecv.at[2], other)

    def across(self, k):
        half, rest = self.buf.shape[1] // 2, k % 2
        piece = self.buf.at[((self.x + NX - 1 + 2 * (k // 2)) % NX) * NC + self.c, pl.ds(pl.multiple_of(rest * half, half), half)]
        send(piece, piece, self.dsend.at[4 + k], self.drecv.at[4 + k], self.place(self.x, 1 - self.c))

    def last(self):
        far, other = self.at(self.xa), self.place(self.x, 1 - self.c)
        landed(self.first(far), self.recv.at[2])
        landed(self.second(far), self.recv.at[3])
        send(far, far, self.dsend.at[3], self.drecv.at[3], other)

    def finish(self):
        for k, at in enumerate((self.x, self.xl, self.xr, self.xa)):
            if self.split and 0 < k < 3:
                half = self.buf.shape[1] // 2
                for j in range(2):
                    landed(self.at(at, 1 - self.c).at[pl.ds(j * half, half)], self.drecv.at[2 + 2 * k + j])
            else:
                landed(self.at(at, 1 - self.c), self.drecv.at[k])

    def drain(self, src):
        landed(src, self.send.at[0])
        landed(src, self.send.at[1])
        landed(src, self.dsend.at[0])
        landed(self.first(self.at(self.xl)), self.send.at[2])
        landed(self.second(self.at(self.xr)), self.send.at[3])
        for k, at in enumerate((self.xl, self.xr, self.xa), 1):
            if self.split and k < 3:
                half = self.buf.shape[1] // 2
                for j in range(2):
                    landed(self.at(at).at[pl.ds(j * half, half)], self.dsend.at[2 + 2 * k + j])
            else:
                landed(self.at(at), self.dsend.at[k])


def attend(qs, m, acc, k, v, sbuf, block, starts):
    n = len(starts)
    width = k.shape[0]
    v1 = jnp.concatenate([v, jnp.ones(v.shape, v.dtype)], axis=1)

    def scores(i):
        return lax.dot_general(qs[pl.ds(starts[i], block), :], k, NT, preferred_element_type=F32)

    sbuf[0, :, :width] = scores(0)
    for i in range(n):
        if i + 1 < n:
            sbuf[(i + 1) % 2, :, :width] = scores(i + 1)
        rows = pl.ds(starts[i], block)
        s = sbuf[i % 2, :, :width]
        before = m[rows, :]
        after = jnp.maximum(before, jnp.max(s, axis=1, keepdims=True))
        p = jnp.exp2(s - after[:, :1]).astype(BF16)
        rescale = jnp.exp2(before - after)
        m[rows, :] = after
        pv = jnp.dot(p, v1, preferred_element_type=F32)
        acc[rows, :] = acc[rows, :] * jnp.concatenate([rescale, rescale], axis=1) + pv


def kernel(
    tok, ctxr,
    lat_h, ctx_h, cl_h, cc_h, shw_h, scw_h, gaw_h, gain_h, lam_h, rowt_h, colt_h, wq, wk, wv, wo, out,
    lat, ctx, cond, modm, small, lam_s, rowt, colt, cos, sin,
    zbuf, ybuf, tbuf, modw, lbuf, hid, w, wall, qst, kst, vst, qbuf, kv, qs, m, acc, sbuf, obuf, hb,
    wsem, zs_s, zs_r, ys_s, ys_r, ts_s, ts_r,
    l_s, l_r, l_ds, l_dr, w_s, w_r, w_ds, w_dr,
    q_s, q_r, k_s, v_s, kv_r, own_s, fwd_s, ring_r, d_s, d_r, o_s, o_r,
):
    sp, tp = lax.axis_index("sp"), lax.axis_index("tp")
    z, y = sp // NY, sp % NY
    x, c = tp // NC, tp % NC

    def place(px, pc, py=None, pz=None):
        return ((z if pz is None else pz) * NY + (y if py is None else py), px * NC + pc)

    pairs = [
        (lat_h, lat), (cl_h, cond.at[pl.ds(0, 1)]), (cc_h, cond.at[pl.ds(1, 1)]),
        (shw_h, modm.at[0]), (scw_h, modm.at[1]), (gaw_h, modm.at[2]),
        (rowt_h, rowt), (colt_h, colt), (ctx_h, ctx), (gain_h, small), (lam_h, lam_s),
        (wk.at[0], w.at[:, pl.ds(256, 128)]), (wk.at[1], w.at[:, pl.ds(384, 128)]),
        (wv, w.at[:, pl.ds(512, 256)]),
        (wq.at[0], w.at[:, pl.ds(0, 128)]), (wq.at[1], w.at[:, pl.ds(128, 128)]),
        (wo, wall.at[tp]),
    ]
    loads = [pltpu.make_async_copy(src, dst, wsem.at[k]) for k, (src, dst) in enumerate(pairs)]

    barrier = pltpu.get_barrier_semaphore()
    others = [(dx, dy, dc) for dx in range(NX) for dy in range(NY) for dc in range(NC)][1:]
    for dz in range(1, NZ):
        pl.semaphore_signal(barrier, inc=1, device_id=place(x, c, pz=(z + dz) % NZ), device_id_type=MESH)
    for dx, dy, dc in others:
        pl.semaphore_signal(
            barrier, inc=1, device_id=place((x + dx) % NX, (c + dc) % NC, py=(y + dy) % NY), device_id_type=MESH
        )
    for load in loads:
        load.start()
    for load in loads[:6]:
        load.wait()

    span = modm.shape[1]
    v = cond[:, pl.ds(pl.multiple_of(sp // 2 * 128, 128), 128)]
    v = v / (1.0 + jnp.exp(-v))
    v = jnp.where(sp % 2 == 0, v, pltpu.roll(v, 128 - span, 1))[:, :span]
    row = lax.broadcasted_iota(jnp.int32, (16, span), 0)
    first, second, none = v[0:1], v[1:2], jnp.zeros((16, span), F32)

    def left(k):
        return jnp.where(row == k, first, jnp.where(row == k + 1, second, none)).astype(BF16)

    part = jnp.dot(left(0), modm[0], preferred_element_type=F32)
    part += jnp.dot(left(2), modm[1], preferred_element_type=F32)
    part += jnp.dot(jnp.where(row == 4, first, none).astype(BF16), modm[2], preferred_element_type=F32)
    zbuf[z] = part[:8]
    lbuf[tp] = lat[...]

    for load in loads[6:11]:
        load.wait()
    in_row = lax.broadcasted_iota(jnp.int32, (GRID_W, 128), 1) % 32 < 16
    for k in range(tok // GRID_W):
        r = sp * (tok // GRID_W) + k
        cos[k * GRID_W : (k + 1) * GRID_W, :] = jnp.where(in_row, rowt[0, pl.ds(r, 1), :], colt[0])
        sin[k * GRID_W : (k + 1) * GRID_W, :] = jnp.where(in_row, rowt[1, pl.ds(r, 1), :], colt[1])
    cos[tok : tok + ctxr, :] = jnp.ones((ctxr, 128), F32)
    sin[tok : tok + ctxr, :] = jnp.zeros((ctxr, 128), F32)
    lines = lax.broadcasted_iota(jnp.int32, (8, 256), 0)
    lane = lax.broadcasted_iota(jnp.int32, (8, 256), 1)
    lam = jnp.where(lane < VALUE_DIM, lam_s[0], lam_s[1])
    extra = jnp.where(lines == 5, small[...], jnp.where(lines == 6, lam, jnp.zeros((8, 256), F32)))

    pl.semaphore_wait(barrier, NZ - 1 + len(others))

    for d in range(1, NZ):
        send(zbuf.at[z], zbuf.at[z], zs_s.at[d - 1], zs_r.at[d - 1], place(x, c, pz=(z + d) % NZ))
    rows = Around(
        lbuf, lambda r: r.at[:, pl.ds(0, 1024)], lambda r: r.at[:, pl.ds(1024, 1024)], (l_s, l_r, l_ds, l_dr), x, c, place
    )
    rows.start(lat)
    for d in range(1, NZ):
        landed(zbuf.at[(z - d + NZ) % NZ], zs_r.at[d - 1])
    total = zbuf[0]
    for k in range(1, NZ):
        total += zbuf[k]
    ybuf[y] = total
    for d in range(1, NY):
        send(ybuf.at[y], ybuf.at[y], ys_s.at[d - 1], ys_r.at[d - 1], place(x, c, py=(y + d) % NY))
    for d in range(1, NY):
        landed(ybuf.at[(y - d + NY) % NY], ys_r.at[d - 1])
    tbuf[tp] = (ybuf[0] + ybuf[1]) + (ybuf[2] + ybuf[3]) + extra
    tps = [(dx, dc) for dx in range(NX) for dc in range(NC)][1:]
    for k, (dx, dc) in enumerate(tps):
        send(tbuf.at[tp], tbuf.at[tp], ts_s.at[k], ts_r.at[k], place((x + dx) % NX, (c + dc) % NC))
    rows.forward()
    for k, (dx, dc) in enumerate(tps):
        landed(tbuf.at[((x - dx + NX) % NX) * NC + (c + dc) % NC], ts_r.at[k])
    for k in range(NX * NC):
        modw[:, k * 256 : (k + 1) * 256] = tbuf[k]
    rows.last()

    loads[16].wait()
    weights = Around(
        wall, lambda r: r.at[pl.ds(0, 128)], lambda r: r.at[pl.ds(128, 128)], (w_s, w_r, w_ds, w_dr), x, c, place, True
    )
    weights.start(wall.at[tp])
    rows.finish()

    def modulate(values, shift, scale):
        values = values.astype(F32)
        inverse = lax.rsqrt(jnp.mean(values * values, axis=-1, keepdims=True) + norm_eps)
        return (values * inverse * (1.0 + scale) + shift).astype(BF16)

    own_rows = lat.shape[0]

    def one_block(k, _):
        hid[pl.ds(pl.multiple_of(k * own_rows, 16), own_rows), :] = modulate(lbuf[k], modw[0:1, :], modw[2:3, :])
        return 0

    lax.fori_loop(0, NX * NC, one_block, 0)
    hid[tok : tok + ctxr, :] = modulate(ctx[...], modw[1:2, :], modw[3:4, :])
    for load in loads[11:16]:
        load.wait()

    lane = lax.broadcasted_iota(jnp.int32, (tok + ctxr, 128), 1)
    low_half, low_head = lane % 64 < 32, lane < 64

    def turned(u):
        swapped = jnp.where(low_half, pltpu.roll(u, 96, 1), pltpu.roll(u, 32, 1))
        return u * cos[...] + swapped * sin[...]

    def by_head(both):
        m1, m2 = turned(both[:, :128]), turned(both[:, 128:])
        return (
            jnp.where(low_head, m1, pltpu.roll(m2, 64, 1)),
            jnp.where(low_head, pltpu.roll(m1, 64, 1), m2),
        )

    keys = by_head(jnp.dot(hid[...], w[:, 256:512], preferred_element_type=F32))
    kst[0], kst[1] = keys[0].astype(BF16), keys[1].astype(BF16)
    vals = jnp.dot(hid[...], w[:, 512:768], preferred_element_type=F32).astype(BF16)
    vst[0], vst[1] = vals[:, :128], vals[:, 128:]

    def self_head(j):
        return 2 * c + j == y

    for j in range(2):
        yd = 2 * c + j
        off = (y - yd + NY) % NY

        @pl.when(jnp.logical_or(yd != y, c != 0))
        def _():
            send(kst.at[j], kv.at[0, z, off], k_s.at[j], kv_r.at[off], place(x, 0, py=yd))

        @pl.when(jnp.logical_and(yd == y, c == 0))
        def _():
            kv[0, z, 0] = kst[j]

        @pl.when(jnp.logical_or(yd != y, c != 1))
        def _():
            send(vst.at[j], kv.at[1, z, off], v_s.at[j], kv_r.at[off], place(x, 1, py=yd))

        @pl.when(jnp.logical_and(yd == y, c == 1))
        def _():
            kv[1, z, 0] = vst[j]

    up, down, other = place(x, c, pz=(z + 1) % NZ), place(x, c, pz=(z + NZ - 1) % NZ), place(x, 1 - c)

    def own(o):
        if o == 0:

            @pl.when(c != y // 2)
            def _():
                landed(kv.at[c, z, 0], kv_r.at[0])
        else:
            landed(kv.at[c, z, o], kv_r.at[o])
        mine = kv.at[c, z, o]
        send(mine, mine, own_s.at[0, o], ring_r.at[0, 0, o], up)
        send(mine, mine, own_s.at[1, o], ring_r.at[1, 0, o], down)
        send(mine, mine, d_s.at[0, o], d_r.at[0, o], other)

    own(0)
    heads = by_head(jnp.dot(hid[...], w[:, 0:256], preferred_element_type=F32))
    for j in range(2):
        qst[j] = (heads[j][:tok] * (log2_e * HEAD_DIM**-0.5)).astype(BF16)
    for j in range(2):
        yd = 2 * c + j

        @pl.when(yd != y)
        def _():
            send(qst.at[j], qbuf.at[y % 2], q_s.at[j], q_r.at[y % 2], place(x, y // 2, py=yd))

        @pl.when(yd == y)
        def _():
            qbuf[y % 2] = qst[j]

    m[...] = jnp.full(m.shape, -jnp.inf, F32)
    acc[...] = jnp.zeros(acc.shape, F32)

    for o in (1, 3, 2):
        own(o)
    for i in range(2):

        @pl.when(2 * c + i != y)
        def _():
            landed(qbuf.at[i], q_r.at[i])

    low = lax.broadcasted_iota(jnp.int32, (tok, 128), 1) < 64
    for i in range(2):
        q = qbuf[i]
        nothing = jnp.zeros_like(q)
        qs[i * tok : (i + 1) * tok, :] = jnp.where(low, q, nothing)
        qs[(2 + i) * tok : (3 + i) * tok, :] = jnp.where(low, nothing, q)
    order = [k * tok + b for k in range(4) for b in range(0, tok, 128)]

    def places(u):
        far, p = (u + 1) // 2, (u + 1) % 2
        return far, p, p * ((u + 6) // 7), ((z - far + NZ) % NZ, (z + far) % NZ)

    def pass_on(u):
        far, p, _, froms = places(u)
        for q in range(2):
            o = 2 * p + q
            for side in range(2):
                piece = kv.at[c, froms[side], o]
                landed(piece, ring_r.at[side, far - 1, o])

                @pl.when(jnp.logical_or(far < 3, p == side))
                def _():
                    send(
                        piece, piece, fwd_s.at[side, far - 1, o], ring_r.at[side, far, o],
                        up if side == 0 else down,
                    )

                send(piece, piece, d_s.at[u, 2 * side + q], d_r.at[u, 2 * side + q], other)

    def unit(u, _):
        @pl.when(u < 6)
        def _():
            pass_on(u + 1)

        @pl.when(u == 3)
        def _():
            weights.forward()

        @pl.when(u >= 3)
        def _():
            weights.across(u - 3)

        _, p, first, froms = places(u)
        for q in range(2):
            landed(kv.at[1 - c, froms[0], 2 * first + q], d_r.at[u, q])
            landed(kv.at[1 - c, froms[1], 2 * p + q], d_r.at[u, 2 + q])
        k, v = (
            jnp.concatenate(
                [
                    kv[part, froms[0], pl.ds(2 * first, 2), 0:tok, :].reshape(2 * tok, 128),
                    kv[part, froms[1], pl.ds(2 * p, 2), 0:tok, :].reshape(2 * tok, 128),
                ]
            )
            for part in range(2)
        )
        attend(qs, m, acc, k, v, sbuf, 128, order)
        return 0

    lax.fori_loop(0, 6, unit, 0)

    def opposite_lands(q):
        for side in range(2):
            piece = kv.at[c, opposite, 2 * side + q]
            landed(piece, ring_r.at[side, 3, 2 * side + q])
            send(piece, piece, d_s.at[7, 2 * side + q], d_r.at[7, 2 * side + q], other)

    opposite = (z + NZ // 2) % NZ
    for q in range(2):
        landed(kv.at[1 - c, (z + 5) % NZ, 2 + q], d_r.at[6, q])
        landed(kv.at[1 - c, (z + 3) % NZ, 2 + q], d_r.at[6, 2 + q])
    k, v = (
        jnp.concatenate(
            [
                kv[part, (z + 5) % NZ, 2:4, 0:tok, :].reshape(2 * tok, 128),
                kv[part, (z + 3) % NZ, 2:4, 0:tok, :].reshape(2 * tok, 128),
            ]
            + [
                kv[part, (opposite + i) % NZ, :, tok : tok + ctxr, :].reshape(NY * ctxr, 128)
                for i in range(1, NZ)
            ]
        )
        for part in range(2)
    )
    opposite_lands(0)
    weights.across(3)
    attend(qs, m, acc, k, v, sbuf, 128, order)

    def finish(i):
        r1, r2 = pl.ds(i * tok, tok), pl.ds((2 + i) * tok, tok)
        mine = tbuf[2 * x + y // 2]
        picked = jnp.where(y % 2 == 0, mine[:, :128], mine[:, 128:])
        gain, factor = picked[5:6, :], picked[6:7, :]
        mixed = acc[r1, :128] / acc[r1, 128:] - factor * (acc[r2, :128] / acc[r2, 128:])
        normed = mixed * lax.rsqrt(jnp.mean(mixed * mixed, axis=-1, keepdims=True) + norm_eps) * gain
        obuf[i] = normed.astype(BF16).reshape(obuf.shape[1:])
        head = NY * x + y
        for t in range(NX * NC):
            home = jnp.logical_and(2 * c + i == y, tp == t)

            @pl.when(jnp.logical_not(home))
            def _():
                send(obuf.at[i, t], hb.at[head], o_s.at[i, t], o_r.at[head], (z * NY + 2 * c + i, t))

            @pl.when(home)
            def _():
                hb[head] = obuf[i, t]

    for q in range(2):
        if q == 0:
            opposite_lands(1)
            weights.last()
        for side in range(2):
            landed(kv.at[1 - c, opposite, 2 * side + q], d_r.at[7, 2 * side + q])
        k, v = (jnp.concatenate([kv[part, opposite, q], kv[part, opposite, 2 + q]]) for part in range(2))
        if q == 0:
            attend(qs, m, acc, k, v, sbuf, 128, order)
        else:
            for i in range(2):
                attend(qs, m, acc, k, v, sbuf, 128, [k2 * tok + b for k2 in (i, 2 + i) for b in range(0, tok, 128)])
                finish(i)
    weights.finish()
    for h in range(NX * NY):
        hx, hy = h // NY, h % NY

        @pl.when(jnp.logical_not(jnp.logical_and(jnp.logical_and(hx == x, hy == y), y // 2 == c)))
        def _():
            landed(hb.at[h], o_r.at[h])

    mixed_sum = jnp.zeros((own_rows, wall.shape[2]), F32)
    for g in range(NX * NC):
        pair = jnp.concatenate([hb[2 * g], hb[2 * g + 1]], axis=1)
        mixed_sum += jnp.dot(pair, wall[g], preferred_element_type=F32).astype(BF16).astype(F32)
    out[...] = modw[4:5, :] * mixed_sum

    for d in range(1, NZ):
        landed(zbuf.at[z], zs_s.at[d - 1])
    for d in range(1, NY):
        landed(ybuf.at[y], ys_s.at[d - 1])
    for k in range(len(tps)):
        landed(tbuf.at[tp], ts_s.at[k])
    rows.drain(lat)
    weights.drain(wall.at[tp])
    for j in range(2):
        yd = 2 * c + j

        @pl.when(yd != y)
        def _():
            landed(qst.at[j], q_s.at[j])

        @pl.when(jnp.logical_or(yd != y, c != 0))
        def _():
            landed(kst.at[j], k_s.at[j])

        @pl.when(jnp.logical_or(yd != y, c != 1))
        def _():
            landed(vst.at[j], v_s.at[j])

    for o in range(NY):
        for side in range(2):
            landed(kv.at[c, z, o], own_s.at[side, o])
            for far in range(3):
                if far < 2 or o // 2 == side:
                    landed(kv.at[c, z, o], fwd_s.at[side, far, o])
        for u in range(NZ):
            landed(kv.at[c, z, o], d_s.at[u, o])
    for i in range(2):
        for t in range(NX * NC):

            @pl.when(jnp.logical_not(jnp.logical_and(2 * c + i == y, tp == t)))
            def _():
                landed(obuf.at[i, t], o_s.at[i, t])


def tables(grid_rows):
    quarter = HEAD_DIM // 4
    inverse = np.float32(rope_theta) ** (-np.arange(quarter, dtype=np.float32) / np.float32(quarter))
    sign = np.array([-1.0, 1.0, -1.0, 1.0]).repeat(2 * quarter)

    def table(count):
        angles = (np.arange(count, dtype=np.float32)[:, None] * inverse).astype(np.float64)
        cos, sin = np.tile(np.cos(angles), (1, 8)), np.tile(np.sin(angles), (1, 8)) * sign
        return jnp.asarray(np.stack([cos, sin]).astype(np.float32))

    return table(grid_rows), table(GRID_W)


def local(
    latent, context, cond_latent, cond_context, shift_weight, scale_weight, gate_weight,
    query_weight, key_weight, value_weight, out_weight, lambda_heads, out_gain,
):
    own_rows, width = latent.shape
    ctxr = context.shape[0]
    tok = own_rows * NX * NC
    rowt, colt = tables(tok * lax.axis_size("sp") // GRID_W)
    hbm = pl.BlockSpec(memory_space=pl.ANY)
    dma = pltpu.SemaphoreType.DMA
    gated = pl.pallas_call(
        functools.partial(kernel, tok, ctxr),
        out_shape=jax.ShapeDtypeStruct((own_rows, width), F32),
        in_specs=[hbm] * 15,
        out_specs=pl.BlockSpec(memory_space=pltpu.VMEM),
        scratch_shapes=[
            pltpu.VMEM((own_rows, width), BF16),
            pltpu.VMEM((ctxr, width), BF16),
            pltpu.VMEM((2, width), F32),
            pltpu.VMEM((3, *shift_weight.shape), BF16),
            pltpu.VMEM((1, 256), F32),
            pltpu.SMEM(lambda_heads.shape, F32),
            pltpu.VMEM(rowt.shape, F32),
            pltpu.VMEM(colt.shape, F32),
            pltpu.VMEM((tok + ctxr, 128), F32),
            pltpu.VMEM((tok + ctxr, 128), F32),
            pltpu.VMEM((NZ, 8, 256), F32),
            pltpu.VMEM((NY, 8, 256), F32),
            pltpu.VMEM((NX * NC, 8, 256), F32),
            pltpu.VMEM((8, width), F32),
            pltpu.VMEM((NX * NC, own_rows, width), BF16),
            pltpu.VMEM((tok + ctxr, width), BF16),
            pltpu.VMEM((width, 768), BF16),
            pltpu.VMEM((NX * NC, 256, width), BF16),
            pltpu.VMEM((2, tok, 128), BF16),
            pltpu.VMEM((2, tok + ctxr, 128), BF16),
            pltpu.VMEM((2, tok + ctxr, 128), BF16),
            pltpu.VMEM((2, tok, 128), BF16),
            pltpu.VMEM((2, NZ, NY, tok + ctxr, 128), BF16),
            pltpu.VMEM((4 * tok, 128), BF16),
            pltpu.VMEM((4 * tok, 128), F32),
            pltpu.VMEM((4 * tok, 256), F32),
            pltpu.VMEM((2, 128, NY * tok + (NZ - 1) * NY * ctxr), F32),
            pltpu.VMEM((2, NX * NC, own_rows, 128), BF16),
            pltpu.VMEM((NX * NY, own_rows, 128), BF16),
            dma((17,)),
            dma((NZ - 1,)), dma((NZ - 1,)), dma((NY - 1,)), dma((NY - 1,)), dma((7,)), dma((7,)),
            dma((4,)), dma((4,)), dma((4,)), dma((4,)),
            dma((4,)), dma((4,)), dma((8,)), dma((8,)),
            dma((2,)), dma((2,)), dma((2,)), dma((2,)), dma((NY,)),
            dma((2, NY)), dma((2, 3, NY)), dma((2, 4, NY)), dma((NZ, NY)), dma((NZ, NY)),
            dma((2, NX * NC)), dma((NX * NY,)),
        ],
        compiler_params=pltpu.CompilerParams(
            collective_id=0, has_side_effects=True, vmem_limit_bytes=60 * 2**20
        ),
    )(
        latent, context, cond_latent[None], cond_context[None], shift_weight, scale_weight, gate_weight,
        out_gain[None], lambda_heads, rowt, colt, query_weight, key_weight, value_weight, out_weight,
    )
    return (latent.astype(F32) + gated).astype(BF16)


def solution(mesh):
    placed = (
        P(("sp", "tp"), None), P("sp", None), P(), P(),
        P("sp", "tp"), P("sp", "tp"), P("sp", "tp"),
        P(None, None, "tp"), P(None, None, "tp"), P(None, "tp"), P("tp", None), P("tp"), P("tp"),
    )
    return jax.shard_map(
        local, mesh=mesh, in_specs=placed, out_specs=P(("sp", "tp"), None), check_vma=False
    )
```

time: 101 us -> 82.2 us (0.81)
  Pallas kernels: 93.5 us -> 80.4 us
  local copies, waits for them, and re-layouts: 3.42 us -> 0.01 us
  other arithmetic: 3.43 us -> 1.71 us
    pallas_call x1, Pallas kernels: 93.5 us -> 80.4 us  [local(): pl.pallas_call(functools.partial(kernel, tok, ctxr), out_shape=jax.ShapeD...]
    unnamed x9 -> x2, local copies, waits for them, and re-layouts: 3.01 us -> 0.01 us
    concatenate x3 -> x0, other arithmetic: 2.44 us -> none  [the longest x1 0.89 us: tables(): cos = jnp.concatenate([cos, cos, cos, cos], axis=-1)]
    convert_element_type x2 -> x1, other arithmetic: 0.09 us -> 1.71 us  [local(): return (latent.astype(F32) + gated).astype(BF16)]
where the time goes in v2:
time: 82.2 us; the launch traced here: 82.1 us
  Pallas kernels  80.4 us (98%)
  other arithmetic  1.71 us (2%)
    pallas_call x1, Pallas kernels, local(): pl.pallas_call(functools.partial(kernel, tok, ctxr), out_shape=jax.ShapeD...  80.4 us
    convert_element_type x1, other arithmetic, local(): return (latent.astype(F32) + gated).astype(BF16)  1.71 us

profile of v2, /device:TPU:1, one launch (start us, length us, event | category | flops | bytes accessed | tf_op | source)
XLA Modules:
  0.0 82.1 jit_solution(16832973512247252030)
XLA Ops:
  0.0 0.0 copy-start
  0.0 80.4 %shard_map.145 = f32[48,2048]{1,0:T(8,128)} custom-call(bf16[48,2048]{1,0:T(8,128)(2,1)} %lat_h.1, bf16[16,2048]{1,0:T(8,128)(2,1)} %ctx_h.1, f32[1,2048]{1,0:T(1,128)} %bitcast.3, f32[1,2048]{1,0:T(1,128)} %bitcast.4, bf16[64,256]{1,0:T(8,128)(2,1)} %shw_h.1, bf16[64,256]{1,0:T(8,128)(2,1)} %scw_h.1, bf16[64,256]{1,0:T(8,128)(2,1)} %gaw_h.1, ...), custom_call_target="tpu_custom_call" | custom-call | tf_op jit(solution)/shard_map/pallas_call | solution.py:525
  80.4 0.0 copy-done
  80.4 1.7 %add_convert_fusion = bf16[48,2048]{1,0:T(8,128)(2,1)} fusion(f32[48,2048]{1,0:T(8,128)} %shard_map.145, bf16[48,2048]{1,0:T(8,128)(2,1)S(1)} %copy-done), kind=kLoop, calls=%fused_computation | loop fusion | flops 294912 | bytes 786432 | tf_op jit(solution)/shard_map/convert_element_type | solution.py:575
Async XLA Ops:
  0.0 80.4 %copy-start = (bf16[48,2048]{1,0:T(8,128)(2,1)S(1)}, bf16[48,2048]{1,0:T(8,128)(2,1)}, u32[]{:S(2)}) copy-start(bf16[48,2048]{1,0:T(8,128)(2,1)} %lat_h.1) | copy-start | bytes 589828

commit v3 on v2

v3 whole, which is shorter than its diff:
```python
import functools

import jax
import jax.numpy as jnp
import numpy as np
from jax import lax
from jax.experimental import pallas as pl
from jax.experimental.pallas import tpu as pltpu
from jax.sharding import PartitionSpec as P

HEAD_DIM = 64
GRID_W = 64
VALUE_DIM = 128
NX, NY, NZ, NC = 4, 4, 8, 2

norm_eps = 1e-06
rope_theta = 10000.0
log2_e = 1.4426950408889634

MESH = pl.DeviceIdType.MESH
F32, BF16 = jnp.float32, jnp.bfloat16
NT = (((1,), (1,)), ((), ()))


def send(src, dst, send_sem, recv_sem, device):
    pltpu.make_async_remote_copy(
        src_ref=src, dst_ref=dst, send_sem=send_sem, recv_sem=recv_sem,
        device_id=device, device_id_type=MESH,
    ).start()


def landed(ref, sem):
    pltpu.make_async_copy(ref, ref, sem).wait()


class Around:
    def __init__(self, buf, first, second, sems, x, c, place, split=False):
        self.split = split
        self.buf, self.first, self.second, self.place = buf, first, second, place
        self.sent, self.recv, self.drecv = sems
        self.c = c
        self.x = x
        self.xl, self.xr, self.xa = (x + 3) % NX, (x + 1) % NX, (x + 2) % NX

    def at(self, x, c=None):
        return self.buf.at[x * NC + (self.c if c is None else c)]

    def start(self, src):
        own, other = self.at(self.x), self.place(self.x, 1 - self.c)
        send(src, own, self.sent, self.recv.at[0], self.place(self.xr, self.c))
        send(src, own, self.sent, self.recv.at[1], self.place(self.xl, self.c))
        send(src, own, self.sent, self.drecv.at[0], other)

    def forward(self):
        left, right = self.at(self.xl), self.at(self.xr)
        landed(left, self.recv.at[0])
        a = self.first(left)
        send(a, a, self.sent, self.recv.at[2], self.place(self.xr, self.c))
        landed(right, self.recv.at[1])
        b = self.second(right)
        send(b, b, self.sent, self.recv.at[3], self.place(self.xl, self.c))

    def near(self):
        left, right, other = self.at(self.xl), self.at(self.xr), self.place(self.x, 1 - self.c)
        send(left, left, self.sent, self.drecv.at[1], other)
        send(right, right, self.sent, self.drecv.at[2], other)

    def across(self, k):
        half, rest = self.buf.shape[1] // 2, k % 2
        piece = self.buf.at[((self.x + NX - 1 + 2 * (k // 2)) % NX) * NC + self.c, pl.ds(pl.multiple_of(rest * half, half), half)]
        send(piece, piece, self.sent, self.drecv.at[4 + k], self.place(self.x, 1 - self.c))

    def last(self):
        far, other = self.at(self.xa), self.place(self.x, 1 - self.c)
        landed(self.first(far), self.recv.at[2])
        landed(self.second(far), self.recv.at[3])
        send(far, far, self.sent, self.drecv.at[3], other)

    def finish(self):
        for k, at in enumerate((self.x, self.xl, self.xr, self.xa)):
            if self.split and 0 < k < 3:
                half = self.buf.shape[1] // 2
                for j in range(2):
                    landed(self.at(at, 1 - self.c).at[pl.ds(j * half, half)], self.drecv.at[2 + 2 * k + j])
            else:
                landed(self.at(at, 1 - self.c), self.drecv.at[k])

    def drain(self):
        landed(self.buf.at[pl.ds(0, 7)], self.sent)


def attend(qs, m, acc, k, v, sbuf, block, starts):
    n = len(starts)
    width = k.shape[0]
    v1 = jnp.concatenate([v, jnp.ones(v.shape, v.dtype)], axis=1)

    def scores(i):
        return lax.dot_general(qs[pl.ds(starts[i], block), :], k, NT, preferred_element_type=F32)

    sbuf[0, :, :width] = scores(0)
    for i in range(n):
        if i + 1 < n:
            sbuf[(i + 1) % 2, :, :width] = scores(i + 1)
        rows = pl.ds(starts[i], block)
        s = sbuf[i % 2, :, :width]
        before = m[rows, :]
        after = jnp.maximum(before, jnp.max(s, axis=1, keepdims=True))
        p = jnp.exp2(s - after[:, :1]).astype(BF16)
        rescale = jnp.exp2(before - after)
        m[rows, :] = after
        pv = jnp.dot(p, v1, preferred_element_type=F32)
        acc[rows, :] = acc[rows, :] * jnp.concatenate([rescale, rescale], axis=1) + pv


def kernel(
    tok, ctxr,
    lat_h, ctx_h, cl_h, cc_h, shw_h, scw_h, gaw_h, gain_h, lam_h, rowt_h, colt_h, wq, wk, wv, wo, out,
    lat, ctx, cond, modm, small, lam_s, rowt, colt, cos, sin,
    zbuf, ybuf, tbuf, modw, inv, lbuf, hid, w, wall, qst, kst, vst, qbuf, kv, qs, m, acc, sbuf, obuf, hb,
    wsem, vec_s, vec_r, gather_s, l_r, l_dr, w_r, w_dr,
    q_s, q_r, k_s, v_s, kv_r, kv_s, ring_r, d_r, o_s, o_r,
):
    sp, tp = lax.axis_index("sp"), lax.axis_index("tp")
    z, y = sp // NY, sp % NY
    x, c = tp // NC, tp % NC

    def place(px, pc, py=None, pz=None):
        return ((z if pz is None else pz) * NY + (y if py is None else py), px * NC + pc)

    pairs = [
        (lat_h, lat), (cl_h, cond.at[pl.ds(0, 1)]), (cc_h, cond.at[pl.ds(1, 1)]),
        (shw_h, modm.at[0]), (scw_h, modm.at[1]), (gaw_h, modm.at[2]),
        (rowt_h, rowt), (colt_h, colt), (ctx_h, ctx), (gain_h, small), (lam_h, lam_s),
        (wk.at[0], w.at[:, pl.ds(256, 128)]), (wk.at[1], w.at[:, pl.ds(384, 128)]),
        (wv, w.at[:, pl.ds(512, 256)]),
        (wq.at[0], w.at[:, pl.ds(0, 128)]), (wq.at[1], w.at[:, pl.ds(128, 128)]),
        (wo, wall.at[tp]),
    ]
    group = [0, 1, 1, 2, 2, 2, 3, 4, 5, 6, 7, 8, 8, 8, 8, 8, 9]
    loads = [pltpu.make_async_copy(src, dst, wsem.at[group[k]]) for k, (src, dst) in enumerate(pairs)]

    barrier = pltpu.get_barrier_semaphore()
    others = [(dx, dy, dc) for dx in range(NX) for dy in range(NY) for dc in range(NC)][1:]
    for dz in range(1, NZ):
        pl.semaphore_signal(barrier, inc=1, device_id=place(x, c, pz=(z + dz) % NZ), device_id_type=MESH)
    for dx, dy, dc in others:
        pl.semaphore_signal(
            barrier, inc=1, device_id=place((x + dx) % NX, (c + dc) % NC, py=(y + dy) % NY), device_id_type=MESH
        )
    for load in loads:
        load.start()
    landed(lat, wsem.at[0])
    landed(cond, wsem.at[1])
    landed(modm, wsem.at[2])

    span = modm.shape[1]
    v = cond[:, pl.ds(pl.multiple_of(sp // 2 * 128, 128), 128)]
    v = v / (1.0 + jnp.exp(-v))
    v = jnp.where(sp % 2 == 0, v, pltpu.roll(v, 128 - span, 1))[:, :span]
    row = lax.broadcasted_iota(jnp.int32, (16, span), 0)
    first, second, none = v[0:1], v[1:2], jnp.zeros((16, span), F32)

    def left(k):
        return jnp.where(row == k, first, jnp.where(row == k + 1, second, none)).astype(BF16)

    part = jnp.dot(left(0), modm[0], preferred_element_type=F32)
    part += jnp.dot(left(2), modm[1], preferred_element_type=F32)
    part += jnp.dot(jnp.where(row == 4, first, none).astype(BF16), modm[2], preferred_element_type=F32)
    zbuf[0] = part[:8]
    lbuf[tp] = lat[...]

    for load in loads[6:11]:
        load.wait()
    in_row = lax.broadcasted_iota(jnp.int32, (GRID_W, 128), 1) % 32 < 16
    for k in range(tok // GRID_W):
        r = sp * (tok // GRID_W) + k
        cos[k * GRID_W : (k + 1) * GRID_W, :] = jnp.where(in_row, rowt[0, pl.ds(r, 1), :], colt[0])
        sin[k * GRID_W : (k + 1) * GRID_W, :] = jnp.where(in_row, rowt[1, pl.ds(r, 1), :], colt[1])
    cos[tok : tok + ctxr, :] = jnp.ones((ctxr, 128), F32)
    sin[tok : tok + ctxr, :] = jnp.zeros((ctxr, 128), F32)
    lines = lax.broadcasted_iota(jnp.int32, (8, 256), 0)
    lane = lax.broadcasted_iota(jnp.int32, (8, 256), 1)
    lam = jnp.where(lane < VALUE_DIM, lam_s[0], lam_s[1])
    extra = jnp.where(lines == 5, small[...], jnp.where(lines == 6, lam, jnp.zeros((8, 256), F32)))

    pl.semaphore_wait(barrier, NZ - 1 + len(others))

    for d in range(1, NZ):
        send(zbuf.at[0], zbuf.at[d], vec_s.at[0], vec_r.at[0], place(x, c, pz=(z + d) % NZ))
    rows = Around(
        lbuf, lambda r: r.at[:, pl.ds(0, 1024)], lambda r: r.at[:, pl.ds(1024, 1024)], (gather_s.at[0], l_r, l_dr), x, c, place
    )
    rows.start(lat)
    landed(zbuf.at[pl.ds(1, NZ - 1)], vec_r.at[0])
    total = zbuf[0]
    for k in range(1, NZ):
        total += zbuf[k]
    ybuf[0] = total
    for d in range(1, NY):
        send(ybuf.at[0], ybuf.at[d], vec_s.at[1], vec_r.at[1], place(x, c, py=(y + d) % NY))
    rows.forward()
    landed(ybuf.at[pl.ds(1, NY - 1)], vec_r.at[1])
    tbuf[tp] = (ybuf[0] + ybuf[1]) + (ybuf[2] + ybuf[3]) + extra
    tps = [(dx, dc) for dx in range(NX) for dc in range(NC)][1:]
    for k, (dx, dc) in enumerate(tps):
        send(tbuf.at[tp], tbuf.at[tp], vec_s.at[2], vec_r.at[2 + k], place((x + dx) % NX, (c + dc) % NC))
    rows.near()
    rows.last()
    loads[16].wait()
    weights = Around(
        wall, lambda r: r.at[pl.ds(0, 128)], lambda r: r.at[pl.ds(128, 128)], (gather_s.at[1], w_r, w_dr), x, c, place, True
    )
    weights.start(wall.at[tp])
    rows.finish()

    def inverse_of(values):
        values = values.astype(F32)
        return lax.rsqrt(jnp.mean(values * values, axis=-1, keepdims=True) + norm_eps)

    def modulate(values, inverse, shift, scale):
        return (values.astype(F32) * inverse * (1.0 + scale) + shift).astype(BF16)

    own_rows = lat.shape[0]

    def one_inverse(k, _):
        rows_of = pl.ds(pl.multiple_of(k * own_rows, 16), own_rows)
        inv[rows_of, :] = jnp.broadcast_to(inverse_of(lbuf[k]), (own_rows, 128))
        return 0

    lax.fori_loop(0, NX * NC, one_inverse, 0)
    inv[tok : tok + ctxr, :] = jnp.broadcast_to(inverse_of(ctx[...]), (ctxr, 128))
    for k, (dx, dc) in enumerate(tps):
        landed(tbuf.at[((x - dx + NX) % NX) * NC + (c + dc) % NC], vec_r.at[2 + k])
    for k in range(NX * NC):
        modw[:, k * 256 : (k + 1) * 256] = tbuf[k]

    def one_block(k, _):
        rows_of = pl.ds(pl.multiple_of(k * own_rows, 16), own_rows)
        hid[rows_of, :] = modulate(lbuf[k], inv[rows_of, :][:, :1], modw[0:1, :], modw[2:3, :])
        return 0

    lax.fori_loop(0, NX * NC, one_block, 0)
    hid[tok : tok + ctxr, :] = modulate(ctx[...], inv[tok : tok + ctxr, :][:, :1], modw[1:2, :], modw[3:4, :])
    landed(w, wsem.at[8])

    lane = lax.broadcasted_iota(jnp.int32, (tok + ctxr, 128), 1)
    low_half, low_head = lane % 64 < 32, lane < 64

    def turned(u):
        swapped = jnp.where(low_half, pltpu.roll(u, 96, 1), pltpu.roll(u, 32, 1))
        return u * cos[...] + swapped * sin[...]

    def by_head(both):
        m1, m2 = turned(both[:, :128]), turned(both[:, 128:])
        return (
            jnp.where(low_head, m1, pltpu.roll(m2, 64, 1)),
            jnp.where(low_head, pltpu.roll(m1, 64, 1), m2),
        )

    near, rest = (y + 1) % 2, y % 2
    ynear, yrest = 2 * c + near, 2 * c + rest
    here = yrest == y

    def to_near(stage, sems, part):
        off = (y - ynear + NY) % NY
        send(stage.at[near], kv.at[part, z, off], sems.at[0], kv_r.at[off], place(x, part, py=ynear))

        @pl.when(jnp.logical_and(here, c == part))
        def _():
            kv[part, z, 0] = stage[rest]

        @pl.when(jnp.logical_and(here, c != part))
        def _():
            send(stage.at[rest], kv.at[part, z, 0], sems.at[1], kv_r.at[0], place(x, part))

    def to_far(stage, sems, part):
        @pl.when(jnp.logical_not(here))
        def _():
            send(stage.at[rest], kv.at[part, z, 2], sems.at[1], kv_r.at[2], place(x, part, py=yrest))

    vals = jnp.dot(hid[...], w[:, 512:768], preferred_element_type=F32).astype(BF16)
    vst[0], vst[1] = vals[:, :128], vals[:, 128:]
    to_near(vst, v_s, 1)
    keys = by_head(jnp.dot(hid[...], w[:, 256:512], preferred_element_type=F32))
    kst[0], kst[1] = keys[0].astype(BF16), keys[1].astype(BF16)
    to_near(kst, k_s, 0)
    to_far(vst, v_s, 1)
    to_far(kst, k_s, 0)

    up, down, other = place(x, c, pz=(z + 1) % NZ), place(x, c, pz=(z + NZ - 1) % NZ), place(x, 1 - c)

    def own(o):
        if o == 0:

            @pl.when(c != y // 2)
            def _():
                landed(kv.at[c, z, 0], kv_r.at[0])
        else:
            landed(kv.at[c, z, o], kv_r.at[o])
        mine = kv.at[c, z, o]
        send(mine, mine, kv_s.at[0], ring_r.at[0, 0, o], up)
        send(mine, mine, kv_s.at[0], ring_r.at[1, 0, o], down)
        send(mine, mine, kv_s.at[2], d_r.at[0, o // 2], other)

    own(0)
    heads = by_head(jnp.dot(hid[...], w[:, 0:256], preferred_element_type=F32))
    for j in range(2):
        qst[j] = (heads[j][:tok] * (log2_e * HEAD_DIM**-0.5)).astype(BF16)
    send(qst.at[near], qbuf.at[y % 2], q_s.at[0], q_r.at[y % 2], place(x, y // 2, py=ynear))

    @pl.when(here)
    def _():
        qbuf[y % 2] = qst[rest]

    @pl.when(jnp.logical_not(here))
    def _():
        send(qst.at[rest], qbuf.at[y % 2], q_s.at[1], q_r.at[y % 2], place(x, y // 2, py=yrest))

    m[...] = jnp.full(m.shape, -jnp.inf, F32)
    acc[...] = jnp.zeros(acc.shape, F32)
    for o in (1, 3, 2):
        own(o)
    for i in range(2):

        @pl.when(2 * c + i != y)
        def _():
            landed(qbuf.at[i], q_r.at[i])

    low = lax.broadcasted_iota(jnp.int32, (tok, 128), 1) < 64
    for i in range(2):
        q = qbuf[i]
        nothing = jnp.zeros_like(q)
        qs[i * tok : (i + 1) * tok, :] = jnp.where(low, q, nothing)
        qs[(2 + i) * tok : (3 + i) * tok, :] = jnp.where(low, nothing, q)
    order = [k * tok + b for k in range(4) for b in range(0, tok, 128)]

    def places(u):
        far, p = (u + 1) // 2, (u + 1) % 2
        return far, p, p * ((u + 6) // 7), ((z - far + NZ) % NZ, (z + far) % NZ)

    def pass_on(u, q):
        far, p, _, froms = places(u)
        o = 2 * p + q
        for side in range(2):
            piece = kv.at[c, froms[side], o]
            landed(piece, ring_r.at[side, far - 1, o])

            @pl.when(jnp.logical_or(far < 3, c == side))
            def _():
                send(piece, piece, kv_s.at[1], ring_r.at[side, far, o], up if side == 0 else down)

            send(piece, piece, kv_s.at[2], d_r.at[u, side], other)

    opposite = (z + NZ // 2) % NZ

    def opposite_lands(p):
        for o in (2 * p, 2 * p + 1):
            piece = kv.at[c, opposite, o]
            landed(piece, ring_r.at[c, 3, o])
            send(piece, piece, kv_s.at[2], d_r.at[7, p], other)

    def unit(u, _):
        @pl.when(u < 6)
        def _():
            pass_on(u + 1, 0)

        @pl.when(u == 6)
        def _():
            opposite_lands(0)

        _, p, first, froms = places(u)
        landed(kv.at[1 - c, froms[0], pl.ds(2 * first, 2)], d_r.at[u, 0])
        landed(kv.at[1 - c, froms[1], pl.ds(2 * p, 2)], d_r.at[u, 1])
        k, v = (
            jnp.concatenate(
                [
                    kv[part, froms[0], pl.ds(2 * first, 2), 0:tok, :].reshape(2 * tok, 128),
                    kv[part, froms[1], pl.ds(2 * p, 2), 0:tok, :].reshape(2 * tok, 128),
                ]
            )
            for part in range(2)
        )
        attend(qs, m, acc, k, v, sbuf, 128, order[:6])
        @pl.when(u < 6)
        def _():
            pass_on(u + 1, 1)

        @pl.when(u == 6)
        def _():
            opposite_lands(1)

        @pl.when(u == 3)
        def _():
            weights.forward()

        @pl.when(u >= 3)
        def _():
            weights.across(u - 3)

        attend(qs, m, acc, k, v, sbuf, 128, order[6:])
        return 0

    lax.fori_loop(0, 7, unit, 0)

    def finish(i):
        r1, r2 = pl.ds(i * tok, tok), pl.ds((2 + i) * tok, tok)
        mine = tbuf[2 * x + y // 2]
        picked = jnp.where(y % 2 == 0, mine[:, :128], mine[:, 128:])
        gain, factor = picked[5:6, :], picked[6:7, :]
        mixed = acc[r1, :128] / acc[r1, 128:] - factor * (acc[r2, :128] / acc[r2, 128:])
        normed = mixed * lax.rsqrt(jnp.mean(mixed * mixed, axis=-1, keepdims=True) + norm_eps) * gain
        obuf[i] = normed.astype(BF16).reshape(obuf.shape[1:])
        head = NY * x + y
        for t in range(NX * NC):
            home = jnp.logical_and(2 * c + i == y, tp == t)

            @pl.when(jnp.logical_not(home))
            def _():
                send(obuf.at[i, t], hb.at[head], o_s.at[0], o_r.at[head // 2], (z * NY + 2 * c + i, t))

            @pl.when(home)
            def _():
                hb[head] = obuf[i, t]

    for p in range(2):
        landed(kv.at[1 - c, opposite, pl.ds(2 * p, 2)], d_r.at[7, p])
    k, v = (
        jnp.concatenate(
            [
                kv[part, opposite, :, 0:tok, :].reshape(NY * tok, 128),
                kv[part, :, :, tok : tok + ctxr, :].reshape(NZ * NY * ctxr, 128),
            ]
        )
        for part in range(2)
    )
    for i in range(2):
        attend(qs, m, acc, k, v, sbuf, 128, [k2 * tok + b for k2 in (i, 2 + i) for b in range(0, tok, 128)])
        finish(i)
        if i == 0:
            weights.last()
    weights.finish()
    mixed_sum = jnp.zeros((own_rows, wall.shape[2]), F32)
    for dx in (0, 1, 3, 2):
        hx = (x + dx) % NX
        for half in range(2):
            g = 2 * hx + half
            if dx == 0:

                @pl.when(jnp.logical_and(c == half, y // 2 == half))
                def _():
                    landed(hb.at[2 * g + 1 - y % 2], o_r.at[g])

                @pl.when(jnp.logical_not(jnp.logical_and(c == half, y // 2 == half)))
                def _():
                    landed(hb.at[pl.ds(2 * g, 2)], o_r.at[g])
            else:
                landed(hb.at[pl.ds(2 * g, 2)], o_r.at[g])
            pair = jnp.concatenate([hb[2 * g], hb[2 * g + 1]], axis=1)
            mixed_sum += jnp.dot(pair, wall[g], preferred_element_type=F32).astype(BF16).astype(F32)
    out[...] = (lat[...].astype(F32) + modw[4:5, :] * mixed_sum).astype(BF16)

    landed(zbuf.at[pl.ds(0, NZ - 1)], vec_s.at[0])
    landed(ybuf.at[pl.ds(0, NY - 1)], vec_s.at[1])
    landed(tbuf.at[pl.ds(0, len(tps))], vec_s.at[2])
    rows.drain()
    weights.drain()
    landed(qst.at[0], q_s.at[0])
    landed(kst.at[0], k_s.at[0])
    landed(vst.at[0], v_s.at[0])

    @pl.when(jnp.logical_not(here))
    def _():
        landed(qst.at[1], q_s.at[1])

    @pl.when(jnp.logical_or(jnp.logical_not(here), c != 0))
    def _():
        landed(kst.at[1], k_s.at[1])

    @pl.when(jnp.logical_or(jnp.logical_not(here), c != 1))
    def _():
        landed(vst.at[1], v_s.at[1])

    landed(kv.at[c, pl.ds(0, 2)], kv_s.at[0])
    landed(kv.at[c, pl.ds(0, 5)], kv_s.at[1])
    landed(kv.at[c], kv_s.at[2])

    @pl.when(c == y // 2)
    def _():
        landed(hb.at[pl.ds(0, NX * NY - 1)], o_s.at[0])

    @pl.when(c != y // 2)
    def _():
        landed(hb, o_s.at[0])


def tables(grid_rows):
    quarter = HEAD_DIM // 4
    inverse = np.float32(rope_theta) ** (-np.arange(quarter, dtype=np.float32) / np.float32(quarter))
    sign = np.array([-1.0, 1.0, -1.0, 1.0]).repeat(2 * quarter)

    def table(count):
        angles = (np.arange(count, dtype=np.float32)[:, None] * inverse).astype(np.float64)
        cos, sin = np.tile(np.cos(angles), (1, 8)), np.tile(np.sin(angles), (1, 8)) * sign
        return jnp.asarray(np.stack([cos, sin]).astype(np.float32))

    return table(grid_rows), table(GRID_W)


def local(
    latent, context, cond_latent, cond_context, shift_weight, scale_weight, gate_weight,
    query_weight, key_weight, value_weight, out_weight, lambda_heads, out_gain,
):
    own_rows, width = latent.shape
    ctxr = context.shape[0]
    tok = own_rows * NX * NC
    rowt, colt = tables(tok * lax.axis_size("sp") // GRID_W)
    hbm = pl.BlockSpec(memory_space=pl.ANY)
    dma = pltpu.SemaphoreType.DMA
    return pl.pallas_call(
        functools.partial(kernel, tok, ctxr),
        out_shape=jax.ShapeDtypeStruct((own_rows, width), BF16),
        in_specs=[hbm] * 15,
        out_specs=pl.BlockSpec(memory_space=pltpu.VMEM),
        scratch_shapes=[
            pltpu.VMEM((own_rows, width), BF16),
            pltpu.VMEM((ctxr, width), BF16),
            pltpu.VMEM((2, width), F32),
            pltpu.VMEM((3, *shift_weight.shape), BF16),
            pltpu.VMEM((1, 256), F32),
            pltpu.SMEM(lambda_heads.shape, F32),
            pltpu.VMEM(rowt.shape, F32),
            pltpu.VMEM(colt.shape, F32),
            pltpu.VMEM((tok + ctxr, 128), F32),
            pltpu.VMEM((tok + ctxr, 128), F32),
            pltpu.VMEM((NZ, 8, 256), F32),
            pltpu.VMEM((NY, 8, 256), F32),
            pltpu.VMEM((NX * NC, 8, 256), F32),
            pltpu.VMEM((8, width), F32),
            pltpu.VMEM((tok + ctxr, 128), F32),
            pltpu.VMEM((NX * NC, own_rows, width), BF16),
            pltpu.VMEM((tok + ctxr, width), BF16),
            pltpu.VMEM((width, 768), BF16),
            pltpu.VMEM((NX * NC, 256, width), BF16),
            pltpu.VMEM((2, tok, 128), BF16),
            pltpu.VMEM((2, tok + ctxr, 128), BF16),
            pltpu.VMEM((2, tok + ctxr, 128), BF16),
            pltpu.VMEM((2, tok, 128), BF16),
            pltpu.VMEM((2, NZ, NY, tok + ctxr, 128), BF16),
            pltpu.VMEM((4 * tok, 128), BF16),
            pltpu.VMEM((4 * tok, 128), F32),
            pltpu.VMEM((4 * tok, 256), F32),
            pltpu.VMEM((2, 128, NY * (tok + NZ * ctxr)), F32),
            pltpu.VMEM((2, NX * NC, own_rows, 128), BF16),
            pltpu.VMEM((NX * NY, own_rows, 128), BF16),
            dma((10,)), dma((3,)), dma((9,)), dma((2,)), dma((4,)), dma((4,)), dma((4,)), dma((8,)),
            dma((2,)), dma((2,)), dma((2,)), dma((2,)), dma((NY,)),
            dma((3,)), dma((2, 4, NY)), dma((NZ, 2)), dma((1,)), dma((NX * NC,)),
        ],
        compiler_params=pltpu.CompilerParams(
            collective_id=0, has_side_effects=True, vmem_limit_bytes=60 * 2**20
        ),
    )(
        latent, context, cond_latent[None], cond_context[None], shift_weight, scale_weight, gate_weight,
        out_gain[None], lambda_heads, rowt, colt, query_weight, key_weight, value_weight, out_weight,
    )


def solution(mesh):
    placed = (
        P(("sp", "tp"), None), P("sp", None), P(), P(),
        P("sp", "tp"), P("sp", "tp"), P("sp", "tp"),
        P(None, None, "tp"), P(None, None, "tp"), P(None, "tp"), P("tp", None), P("tp"), P("tp"),
    )
    return jax.shard_map(
        local, mesh=mesh, in_specs=placed, out_specs=P(("sp", "tp"), None), check_vma=False
    )
```

time: 82.2 us -> 75.8 us (0.922)
  Pallas kernels: 80.4 us -> 73.9 us
  other arithmetic: 1.71 us -> 0 us
  local copies, waits for them, and re-layouts: 0.01 us -> 1.62 us
    pallas_call x1, Pallas kernels: 80.4 us -> 73.9 us  [local(): pl.pallas_call(functools.partial(kernel, tok, ctxr), out_shape=jax.ShapeD...]
    convert_element_type x1 -> x0, other arithmetic: 1.71 us -> none  [local(): return (latent.astype(F32) + gated).astype(BF16)]
    unnamed x2 -> x1, local copies, waits for them, and re-layouts: 0.01 us -> 1.62 us
where the time goes in v3:
time: 75.8 us; the launch traced here: 75.5 us
  Pallas kernels  73.9 us (97%)
  local copies, waits for them, and re-layouts  1.62 us (2%)
    pallas_call x1, Pallas kernels, local(): pl.pallas_call(functools.partial(kernel, tok, ctxr), out_shape=jax.ShapeD...  73.9 us
    unnamed x1, local copies, waits for them, and re-layouts  1.62 us

profile of v3, /device:TPU:1, one launch (start us, length us, event | category | flops | bytes accessed | tf_op | source)
XLA Modules:
  0.0 75.5 jit_solution(7910083849981834906)
XLA Ops:
  0.0 73.9 %shard_map.145 = bf16[48,2048]{1,0:T(8,128)(2,1)} custom-call(bf16[48,2048]{1,0:T(8,128)(2,1)} %lat_h.1, bf16[16,2048]{1,0:T(8,128)(2,1)} %ctx_h.1, f32[1,2048]{1,0:T(1,128)} %bitcast.3, f32[1,2048]{1,0:T(1,128)} %bitcast.4, bf16[64,256]{1,0:T(8,128)(2,1)} %shw_h.1, bf16[64,256]{1,0:T(8,128)(2,1)} %scw_h.1, bf16[64,256]{1,0:T(8,128)(2,1)} %gaw_h.1, ...), custom_call_target="tpu_custom_call" | custom-call | tf_op jit(solution)/shard_map/pallas_call | solution.py:519
  73.9 1.6 %copy.17 = bf16[48,2048]{1,0:T(8,128)(2,1)} copy(bf16[48,2048]{1,0:T(8,128)(2,1)} %shard_map.145) | data formatting | bytes 393216

commit v4 on v3

--- a/solution.py
+++ b/solution.py
@@ -205,29 +205,40 @@
     for k, (dx, dc) in enumerate(tps):
         send(tbuf.at[tp], tbuf.at[tp], vec_s.at[2], vec_r.at[2 + k], place((x + dx) % NX, (c + dc) % NC))
     rows.near()
+    own_rows = lat.shape[0]
+
+    def inverse_of(values):
+        values = values.astype(F32)
+        return lax.rsqrt(jnp.mean(values * values, axis=-1, keepdims=True) + norm_eps)
+
+    def one_inverse(k):
+        rows_of = pl.ds(pl.multiple_of(k * own_rows, 16), own_rows)
+        inv[rows_of, :] = jnp.broadcast_to(inverse_of(lbuf[k]), (own_rows, 128))
+
+    def three(k, _):
+        one_inverse((x + NX - 1 + k) % NX * NC + c)
+        return 0
+
+    def four(k, _):
+        one_inverse(k * NC + 1 - c)
+        return 0
+
+    lax.fori_loop(0, 3, three, 0)
     rows.last()
+    rows.finish()
+
     loads[16].wait()
     weights = Around(
         wall, lambda r: r.at[pl.ds(0, 128)], lambda r: r.at[pl.ds(128, 128)], (gather_s.at[1], w_r, w_dr), x, c, place, True
     )
     weights.start(wall.at[tp])
-    rows.finish()
-
-    def inverse_of(values):
-        values = values.astype(F32)
-        return lax.rsqrt(jnp.mean(values * values, axis=-1, keepdims=True) + norm_eps)
 
     def modulate(values, inverse, shift, scale):
         return (values.astype(F32) * inverse * (1.0 + scale) + shift).astype(BF16)
 
-    own_rows = lat.shape[0]
-
-    def one_inverse(k, _):
-        rows_of = pl.ds(pl.multiple_of(k * own_rows, 16), own_rows)
-        inv[rows_of, :] = jnp.broadcast_to(inverse_of(lbuf[k]), (own_rows, 128))
-        return 0
-
-    lax.fori_loop(0, NX * NC, one_inverse, 0)
+
+    one_inverse((x + 2) % NX * NC + c)
+    lax.fori_loop(0, NX, four, 0)
     inv[tok : tok + ctxr, :] = jnp.broadcast_to(inverse_of(ctx[...]), (ctxr, 128))
     for k, (dx, dc) in enumerate(tps):
         landed(tbuf.at[((x - dx + NX) % NX) * NC + (c + dc) % NC], vec_r.at[2 + k])

time: 75.8 us -> 75.5 us (level)
  no operation moved by 1% of the time
where the time goes in v4:
time: 75.5 us; the launch traced here: 74.8 us
  Pallas kernels  73.2 us (97%)
  local copies, waits for them, and re-layouts  1.62 us (2%)
    pallas_call x1, Pallas kernels, local(): pl.pallas_call(functools.partial(kernel, tok, ctxr), out_shape=jax.ShapeD...  73.2 us
    unnamed x1, local copies, waits for them, and re-layouts  1.62 us

profile of v4, /device:TPU:1, one launch (start us, length us, event | category | flops | bytes accessed | tf_op | source)
XLA Modules:
  0.0 74.8 jit_solution(637470287214633454)
XLA Ops:
  0.0 73.2 %shard_map.145 = bf16[48,2048]{1,0:T(8,128)(2,1)} custom-call(bf16[48,2048]{1,0:T(8,128)(2,1)} %lat_h.1, bf16[16,2048]{1,0:T(8,128)(2,1)} %ctx_h.1, f32[1,2048]{1,0:T(1,128)} %bitcast.3, f32[1,2048]{1,0:T(1,128)} %bitcast.4, bf16[64,256]{1,0:T(8,128)(2,1)} %shw_h.1, bf16[64,256]{1,0:T(8,128)(2,1)} %scw_h.1, bf16[64,256]{1,0:T(8,128)(2,1)} %gaw_h.1, ...), custom_call_target="tpu_custom_call" | custom-call | tf_op jit(solution)/shard_map/pallas_call | solution.py:530
  73.2 1.6 %copy.17 = bf16[48,2048]{1,0:T(8,128)(2,1)} copy(bf16[48,2048]{1,0:T(8,128)(2,1)} %shard_map.145) | data formatting | bytes 393216
